TPU v7x, 32 devices: a whole 2x2x4 slice. The times are simulated.
32 devices in a mesh: rep: 4 (over z), fs: 2 (over y), tp: 4 (over x, core).
Axes of the slice: x: 2, y: 2, z: 4, core: 2. Of those that a mesh axis runs over, the one named last changes fastest.
Arguments:
- tokens: bfloat16 [1536, 2048], P('rep', ('fs', 'tp')), may hold values from -6 to 6
- cotangent: bfloat16 [1536, 2048], P('rep', ('fs', 'tp')), may hold values from -6 to 6
- gain: float32 [2048], replicated, may hold values from 0.1 to 1.9
- w_gate: bfloat16 [5376, 2048], P(('fs', 'tp')), may hold values from -0.125 to 0.125
- w_up: bfloat16 [5376, 2048], P(('fs', 'tp')), may hold values from -0.125 to 0.125
- w_down: bfloat16 [5376, 2048], P(('fs', 'tp')), may hold values from -0.078125 to 0.078125
Outputs:
- grad_input: bfloat16 [1536, 2048], P('rep', ('fs', 'tp'))
- grad_gain: float32 [2048], P(('fs', 'tp'))
- grad_gate: float32 [5376, 2048], P(('fs', 'tp'))
- grad_up: float32 [5376, 2048], P(('fs', 'tp'))
- grad_down: float32 [5376, 2048], P(('fs', 'tp'))
All inputs are finite; a program needn't handle non-finite values.
Results may differ from a plain program's by a relative error of at most 0.006.
Values may be sent and summed in bfloat16 or wider, within the bound.
A program may use at most 128 MiB of HBM per device.

v0:
```python
import functools

import jax
import jax.numpy as jnp
from jax import lax
from jax.experimental import pallas as pl
from jax.experimental.pallas import tpu as pltpu
from jax.sharding import PartitionSpec as P

EPS = 1e-06
PLANE = ("fs", "tp")


def right_product(left, weight):
    return lax.dot_general(
        left, weight, (((1,), (1,)), ((), ())), preferred_element_type=jnp.float32
    )


def left_product(left, right):
    return lax.dot_general(
        left, right, (((0,), (0,)), ((), ())), preferred_element_type=jnp.float32
    )


def normalise(x, gain):
    xf = x.astype(jnp.float32)
    inv_rms = lax.rsqrt(jnp.mean(xf * xf, axis=1, keepdims=True) + EPS)
    return inv_rms, (xf * inv_rms * gain).astype(jnp.bfloat16)


def hidden_grads(normed, dy, w_gate, w_up, w_down):
    gate = right_product(normed, w_gate)
    up = right_product(normed, w_up)
    sig = jax.nn.sigmoid(gate)
    active = gate * sig
    hidden = (active * up).astype(jnp.bfloat16)
    d_hidden = 0.5 * right_product(dy, w_down)
    d_gate = (d_hidden * up * sig * (1.0 + gate * (1.0 - sig))).astype(jnp.bfloat16)
    d_up = (d_hidden * active).astype(jnp.bfloat16)
    return hidden, d_gate, d_up


def hidden_sum(d_gate, d_up, w_gate, w_up):
    return jnp.dot(d_gate, w_gate, preferred_element_type=jnp.float32) + jnp.dot(
        d_up, w_up, preferred_element_type=jnp.float32
    )


def axis_sums(rows_part, gain_part):
    return lax.psum(rows_part, PLANE), lax.psum(gain_part, "rep")


def input_grads(tokens, cotangent, gain, inv_rms, partial_value, sums):
    width = partial_value.shape[1]
    summed = lax.psum_scatter(
        partial_value, PLANE, scatter_dimension=1, tiled=True
    ).astype(jnp.float32)
    own_width = summed.shape[1]
    unit_own = tokens.astype(jnp.float32) * inv_rms
    gain_own = lax.dynamic_slice_in_dim(
        gain, lax.axis_index(PLANE) * own_width, own_width, 0
    )
    d_unit = summed * gain_own
    row_sum, gain_part = sums(jnp.sum(unit_own * d_unit, axis=1), jnp.sum(unit_own * summed, axis=0))
    row_mean = row_sum / width
    grad_input = (
        cotangent.astype(jnp.float32) + inv_rms * (d_unit - unit_own * row_mean[:, None])
    ).astype(jnp.bfloat16)
    return grad_input, gain_part


def reduced(tokens, cotangent, gain, w_gate, w_up, w_down):
    full_x = lax.all_gather(tokens, PLANE, axis=1, tiled=True)
    full_dy = lax.all_gather(cotangent, PLANE, axis=1, tiled=True)
    inv_rms, normed = normalise(full_x, gain)
    hidden, d_gate, d_up = hidden_grads(normed, full_dy, w_gate, w_up, w_down)
    grad_down = 0.5 * left_product(hidden, full_dy)
    grad_gate = left_product(d_gate, normed)
    grad_up = left_product(d_up, normed)
    grad_input, gain_part = input_grads(
        tokens, cotangent, gain, inv_rms, hidden_sum(d_gate, d_up, w_gate, w_up),
        lambda rows_part, gain_part: (lax.psum(rows_part, PLANE), gain_part),
    )
    grad_gate, grad_up, grad_down, grad_gain = lax.psum(
        (grad_gate, grad_up, grad_down, gain_part), "rep"
    )
    return (grad_input, grad_gain, grad_gate, grad_up, grad_down)


def gather_kernel(reps, tps, x_ref, dy_ref, out_ref, buf, send_sem, recv_sem, pair_sem, in_sem, out_sem):
    z, y, t = lax.axis_index("rep"), lax.axis_index("fs"), lax.axis_index("tp")
    rows, cols = x_ref.shape
    x_id = (z, y, lax.rem(t + 2, tps))
    y_id = (z, 1 - y, t)
    pair_id = (z, y, t + 1 - 2 * lax.rem(t, 2))
    up_id, down_id = (z + 1, y, t), (z - 1, y, t)
    has_up, has_down = z < reps - 1, z > 0
    column = (
        y * tps + t,
        y * tps + lax.rem(t + 2, tps),
        (1 - y) * tps + t,
        (1 - y) * tps + lax.rem(t + 2, tps),
    )
    pair_column = tuple(c + 1 - 2 * lax.rem(t, 2) for c in column)

    def piece(level, col, p):
        return buf.at[
            p,
            pl.ds(pl.multiple_of(level * rows, rows), rows),
            pl.ds(pl.multiple_of(col * cols, cols), cols),
        ]

    def copy(level, q, p, kind, target, landing):
        ref = piece(level, column[q], p)
        return pltpu.make_async_remote_copy(
            src_ref=ref, dst_ref=ref, send_sem=send_sem.at[kind, level, p], recv_sem=landing,
            device_id=target, device_id_type=pl.DeviceIdType.MESH,
        )

    def to_x(level, p):
        return copy(level, 0, p, 0, x_id, recv_sem.at[1, level, p])

    def to_y(level, p):
        return copy(level, 0, p, 1, y_id, recv_sem.at[2, level, p])

    def to_pair(level, q, p):
        return copy(level, q, p, 2 + q, pair_id, pair_sem.at[q, level, p])

    def to_up(level, p):
        return copy(level, 0, p, 6, up_id, recv_sem.at[0, level, p])

    def to_down(level, p):
        return copy(level, 0, p, 7, down_id, recv_sem.at[0, level, p])

    def corner(level, p):
        if p == 0:
            return copy(level, 1, p, 8, y_id, recv_sem.at[3, level, p])
        return copy(level, 2, p, 8, x_id, recv_sem.at[3, level, p])

    def landed(level, q, p):
        copy(level, q, p, 0, x_id, recv_sem.at[q, level, p]).wait_recv()

    loads = [
        pltpu.make_async_copy(ref, piece(z, column[0], p), in_sem.at[p])
        for p, ref in enumerate((x_ref, dy_ref))
    ]
    for load in loads:
        load.start()
    barrier = pltpu.get_barrier_semaphore()

    def greet(target):
        pl.semaphore_signal(barrier, inc=1, device_id=target, device_id_type=pl.DeviceIdType.MESH)

    for target in (x_id, y_id, pair_id):
        greet(target)
    pl.when(has_up)(lambda: greet(up_id))
    pl.when(has_down)(lambda: greet(down_id))
    along_z = lax.div(z + reps - 1, reps) + lax.div(2 * reps - 2 - z, reps)
    pl.semaphore_wait(barrier, 3 + along_z)

    for p in range(2):
        loads[p].wait()
        pl.when(has_up)(lambda p=p: to_up(z, p).start())
        pl.when(has_down)(lambda p=p: to_down(z, p).start())
        to_x(z, p).start()
        to_y(z, p).start()
        to_pair(z, 0, p).start()

    for far in range(1, reps):
        for p in range(2):

            @pl.when(z + far < reps)
            def _():
                level = z + far
                landed(level, 0, p)
                pl.when(has_down)(lambda: to_down(level, p).start())
                to_x(level, p).start()
                to_y(level, p).start()
                to_pair(level, 0, p).start()

            @pl.when(z - far >= 0)
            def _():
                level = z - far
                landed(level, 0, p)
                pl.when(has_up)(lambda: to_up(level, p).start())
                to_x(level, p).start()
                to_y(level, p).start()
                to_pair(level, 0, p).start()

    def each_level(act):
        act(z)
        for far in range(1, reps):
            pl.when(z + far < reps)(lambda far=far: act(z + far))
            pl.when(z - far >= 0)(lambda far=far: act(z - far))

    def relay(level):
        for q, p in ((1, 0), (2, 0), (1, 1), (2, 1)):
            landed(level, q, p)
            if q == p + 1:
                corner(level, p).start()
            to_pair(level, q, p).start()

    def corners(level):
        for p in range(2):
            landed(level, 3, p)
            to_pair(level, 3, p).start()

    def store(level, p):
        window = pl.ds(pl.multiple_of(level * rows, rows), rows)
        return pltpu.make_async_copy(
            buf.at[p, window], out_ref.at[p, window], out_sem.at[level, p]
        )

    def finish(level):
        for p in range(2):
            for q in range(4):
                ref = piece(level, pair_column[q], p)
                pltpu.make_async_remote_copy(
                    src_ref=ref, dst_ref=ref, send_sem=send_sem.at[2 + q, level, p],
                    recv_sem=pair_sem.at[q, level, p],
                    device_id=pair_id, device_id_type=pl.DeviceIdType.MESH,
                ).wait_recv()
            store(level, p).start()

    def drain(level):
        for p in range(2):
            to_x(level, p).wait_send()
            to_y(level, p).wait_send()
            corner(level, p).wait_send()
            for q in range(4):
                to_pair(level, q, p).wait_send()
            pl.when(jnp.logical_and(has_up, level <= z))(lambda p=p: to_up(level, p).wait_send())
            pl.when(jnp.logical_and(has_down, level >= z))(lambda p=p: to_down(level, p).wait_send())
            store(level, p).wait()

    for act in (relay, corners, finish, drain):
        each_level(act)


def gather_all(tokens, cotangent):
    reps, fss, tps = (lax.axis_size(name) for name in ("rep", "fs", "tp"))
    rows, cols = tokens.shape
    shape = (2, reps * rows, fss * tps * cols)
    return pl.pallas_call(
        functools.partial(gather_kernel, reps, tps),
        out_shape=jax.ShapeDtypeStruct(shape, tokens.dtype),
        in_specs=[pl.BlockSpec(memory_space=pl.ANY)] * 2,
        out_specs=pl.BlockSpec(memory_space=pl.ANY),
        scratch_shapes=[
            pltpu.VMEM(shape, tokens.dtype),
            pltpu.SemaphoreType.DMA((9, reps, 2)),
            pltpu.SemaphoreType.DMA((4, reps, 2)),
            pltpu.SemaphoreType.DMA((4, reps, 2)),
            pltpu.SemaphoreType.DMA((2,)),
            pltpu.SemaphoreType.DMA((reps, 2)),
        ],
        compiler_params=pltpu.CompilerParams(
            collective_id=0, has_side_effects=True, vmem_limit_bytes=48 * 2**20
        ),
    )(tokens, cotangent)


def gathered(tokens, cotangent, gain, w_gate, w_up, w_down):
    rows, cols = tokens.shape
    if (lax.axis_size("fs"), lax.axis_size("tp")) == (2, 4) and cols % 128 == 0:
        both = gather_all(tokens, cotangent)
    else:
        reps, plane = lax.axis_size("rep"), lax.axis_size(PLANE)
        both = lax.all_gather(jnp.stack([tokens, cotangent]), ("rep",) + PLANE)
        both = both.reshape(reps, plane, 2, rows, cols).transpose(2, 0, 3, 1, 4)
        both = both.reshape(2, reps * rows, plane * cols)
    inv_rms, normed = normalise(both[0], gain)
    dy = both[1]
    hidden, d_gate, d_up = hidden_grads(normed, dy, w_gate, w_up, w_down)
    start = lax.axis_index("rep") * rows
    own = lambda a: lax.dynamic_slice_in_dim(a, start, rows, 0)
    partial_value = hidden_sum(own(d_gate), own(d_up), w_gate, w_up).astype(jnp.bfloat16)
    partial_value, hidden, d_gate, d_up = lax.optimization_barrier(
        (partial_value, hidden, d_gate, d_up)
    )
    grad_input, grad_gain = input_grads(
        tokens, cotangent, gain, own(inv_rms), partial_value, axis_sums
    )
    grad_down = 0.5 * left_product(hidden, dy)
    grad_gate = left_product(d_gate, normed)
    grad_up = left_product(d_up, normed)
    return (grad_input, grad_gain, grad_gate, grad_up, grad_down)


def local(tokens, cotangent, gain, w_gate, w_up, w_down):
    reps = lax.axis_size("rep")
    token_bytes = 2 * 2 * tokens.shape[0] * reps * w_gate.shape[1]
    grad_bytes = 3 * 4 * w_gate.size
    plan = gathered if token_bytes < grad_bytes else reduced
    return plan(tokens, cotangent, gain, w_gate, w_up, w_down)


def solution(mesh):
    placed = (
        P("rep", PLANE),
        P("rep", PLANE),
        P(),
        P(PLANE, None),
        P(PLANE, None),
        P(PLANE, None),
    )
    return jax.shard_map(
        local,
        mesh=mesh,
        in_specs=placed,
        out_specs=(
            P("rep", PLANE),
            P(PLANE),
            P(PLANE, None),
            P(PLANE, None),
            P(PLANE, None),
        ),
        check_vma=False,
    )
```

profile of v0, /device:TPU:0, one launch (start us, length us, event | category | flops | bytes accessed | tf_op | source)
XLA Modules:
  0.0 178.2 jit_solution(11787138568260206092)
XLA Ops:
  7.2 0.0 copy-start
  7.2 0.0 reduce-scatter.2.cloned.1.call-start
  7.2 0.0 copy-start.1
  7.2 1.1 copy-done.1
  8.3 0.0 copy-start.3
  8.3 0.9 copy-done.3
  9.2 61.6 %shard_map.101 = bf16[2,1536,2048]{2,1,0:T(8,128)(2,1)} custom-call(bf16[384,256]{1,0:T(8,128)(2,1)S(1)} %copy-done.1, bf16[384,256]{1,0:T(8,128)(2,1)S(1)} %copy-done.3), custom_call_target="tpu_custom_call" | custom-call | tf_op jit(solution)/shard_map/pallas_call | solution.py:245
  70.8 0.0 copy-start.10
  70.9 4.2 %fusion = f32[1536]{0:T(1024)S(1)} fusion(bf16[2,1536,2048]{2,1,0:T(8,128)(2,1)} %shard_map.101), kind=kLoop, calls=%fused_computation.2 | loop fusion | flops 9435648 | bytes 6297600 | tf_op jit(solution)/shard_map/reduce_sum | solution.py:28
  75.1 0.0 copy-done.10
  75.1 0.0 copy-start.9
  75.1 8.8 %fusion.5 = f32[1536,672]{0,1:T(8,128)} fusion(bf16[672,2048]{1,0:T(8,128)(2,1)S(1)} %copy-done.10, bf16[2,1536,2048]{2,1,0:T(8,128)(2,1)} %shard_map.101), kind=kOutput, calls=%fused_computation.7 | convolution fusion | flops 4227858432 | bytes 13172736 | tf_op jit(solution)/shard_map/dot_general | solution.py:15
  83.9 0.0 copy-done.9
  83.9 0.0 copy-start.11
  83.9 7.8 %fusion.29 = f32[1536,672]{0,1:T(8,128)S(1)} fusion(bf16[672,2048]{1,0:T(8,128)(2,1)} %param.9, f32[2048]{0:T(1024)S(1)} %copy-done.9, f32[1536]{0:T(1024)S(1)} %add_rsqrt_fusion, bf16[2,1536,2048]{2,1,0:T(8,128)(2,1)} %shard_map.101), kind=kOutput, calls=%fused_computation.37 | convolution fusion | flops 4240441344 | bytes 13187072 | tf_op jit(solution)/shard_map/dot_general | solution.py:15
  91.7 0.0 copy-done
  91.7 0.0 copy-done.11
  91.7 0.0 copy-start.5
  91.8 9.4 %multiply_convert_fusion = (bf16[1536,672]{0,1:T(8,128)(2,1)}, bf16[1536,672]{0,1:T(8,128)(2,1)S(1)}, bf16[1536,672]{0,1:T(8,128)(2,1)S(1)}) fusion(f32[1536,672]{0,1:T(8,128)S(1)} %fusion.29, f32[1536,672]{0,1:T(8,128)S(1)} %copy-done.11, bf16[672,2048]{1,0:T(8,128)(2,1)S(1)} %copy-done, f32[2048]{0:T(1024)S(1)} %copy-done.9, f32[1536]{0:T(1024)S(1)} %add_rsqrt_fusion, ...), kind=kOutput, calls=%fused_computation.11 | convolution fusion | flops 4256956416 | bytes 23508992 | tf_op jit(solution)/shard_map/dot_general | solution.py:15
  101.2 0.0 copy-start.8
  101.2 0.0 copy-start.6
  101.2 0.0 copy-done.5
  101.2 1.4 fusion.14
  102.6 0.0 copy-done.8
  102.6 0.5 copy-done.6
  103.1 2.7 %add_convert_fusion = bf16[384,2048]{1,0:T(8,128)(2,1)} fusion(f32[384,2048]{1,0:T(8,128)S(1)} %fusion.14, bf16[672,2048]{1,0:T(8,128)(2,1)S(1)} %copy-done, bf16[1536,672]{0,1:T(8,128)(2,1)S(1)} %get-tuple-element.11, s32[]{:T(128)S(6)} %select_n.8), kind=kOutput, calls=%fused_computation.17 | convolution fusion | flops 1058537472 | bytes 7987204 | tf_op jit(solution)/shard_map/dot_general | solution.py:45
  105.8 0.0 reduce-scatter.2.cloned.1.call-update
  105.8 10.3 %fusion.10 = f32[672,2048]{1,0:T(8,128)} fusion(bf16[1536,672]{0,1:T(8,128)(2,1)} %get-tuple-element.12, bf16[2,1536,2048]{2,1,0:T(8,128)(2,1)} %shard_map.101), kind=kOutput, calls=%fused_computation.16 | convolution fusion | flops 4229234688 | bytes 13860864 | tf_op jit(solution)/shard_map/dot_general | solution.py:21
  116.1 0.1 dynamic-slice.3
  116.2 0.1 dynamic_slice.12
  116.2 0.0 copy-start.7
  116.2 10.7 %fusion.27 = f32[672,2048]{1,0:T(8,128)} fusion(bf16[1536,672]{0,1:T(8,128)(2,1)} %copy-done.8, f32[2048]{0:T(1024)S(1)} %copy-done.9, f32[1536]{0:T(1024)S(1)} %add_rsqrt_fusion, bf16[2,1536,2048]{2,1,0:T(8,128)(2,1)} %shard_map.101), kind=kOutput, calls=%fused_computation.36 | convolution fusion | flops 4240441344 | bytes 13875200 | tf_op jit(solution)/shard_map/dot_general | solution.py:21
  127.0 0.0 copy-done.7
  127.0 0.0 copy-start.2
  127.0 0.0 copy-start.4
  127.0 10.0 %fusion.25 = f32[672,2048]{1,0:T(8,128)} fusion(bf16[1536,672]{0,1:T(8,128)(2,1)S(1)} %copy-done.7, f32[2048]{0:T(1024)S(1)} %copy-done.9, f32[1536]{0:T(1024)S(1)} %add_rsqrt_fusion, bf16[2,1536,2048]{2,1,0:T(8,128)(2,1)} %shard_map.101), kind=kOutput, calls=%fused_computation.35 | convolution fusion | flops 4240441344 | bytes 13875200 | tf_op jit(solution)/shard_map/dot_general | solution.py:21
  137.0 7.3 %reduce-scatter.2.cloned.1.call-done = bf16[384,256]{1,0:T(8,128)(2,1)} async-done(((bf16[384,2048]{1,0:T(8,128)(2,1)}), bf16[384,256]{1,0:T(8,128)(2,1)}) %reduce-scatter.2.cloned.1.call-update) | async-done | bytes 196624 | tf_op jit(solution)/shard_map/reduce_scatter | solution.py:56
  144.3 0.0 copy-done.2
  144.3 1.2 fusion.22
  145.5 12.2 %psum.15 = f32[256]{0:T(256)} all-reduce(f32[256]{0:T(256)S(1)} %get-tuple-element.13), channel_id=1, replica_groups=mesh['rep'=4,'fs'=2,'tp'=4] {'rep'}, use_global_device_ids=true, to_apply=%region_5.0 | all-reduce | flops 256 | bytes 2048 | tf_op jit(solution)/shard_map/psum | solution.py:51
  157.7 11.8 %psum.14 = f32[384]{0:T(512)S(1)} all-reduce(f32[384]{0:T(512)S(1)} %get-tuple-element.14), channel_id=1, replica_groups=mesh['rep'=4,'fs'=2,'tp'=4] {'fs','tp'}, use_global_device_ids=true, to_apply=%region_3.0 | all-reduce | flops 384 | bytes 3072 | tf_op jit(solution)/shard_map/psum | solution.py:51
  169.5 0.0 copy-done.4
  169.5 1.8 %fusion.21 = bf16[384,256]{1,0:T(8,128)(2,1)} fusion(bf16[384,256]{1,0:T(8,128)(2,1)} %reduce-scatter.2.cloned.1.call-done, bf16[384,256]{1,0:T(8,128)(2,1)S(1)} %copy-done.2, bf16[384,256]{1,0:T(8,128)(2,1)S(1)} %copy-done.4, f32[384]{0:T(512)S(1)} %broadcast_multiply_fusion, f32[256]{0:T(256)S(1)} %dynamic_slice.12, f32[384]{0:T(512)S(1)} %dynamic-slice.3), kind=kLoop, calls=%fused_computation.28 | loop fusion | flops 983040 | bytes 790528 | tf_op jit(solution)/shard_map/convert_element_type | solution.py:69
  (2 shorter events, 0.0 us)
Async XLA Ops:
  7.2 84.6 %copy-start = (bf16[672,2048]{1,0:T(8,128)(2,1)S(1)}, bf16[672,2048]{1,0:T(8,128)(2,1)}, u32[]{:S(2)}) copy-start(bf16[672,2048]{1,0:T(8,128)(2,1)} %param.10) | copy-start | bytes 8257540
  7.2 137.1 %reduce-scatter.2.cloned.1.call-start = ((), (), s32[]{:S(2)}) async-start(), calls=%async_computation.1 | async-start | bytes 1769472 | tf_op jit(solution)/shard_map/reduce_scatter | solution.py:56
  7.2 1.1 copy-start.1
  8.3 0.9 copy-start.3
  70.8 4.3 %copy-start.10 = (bf16[672,2048]{1,0:T(8,128)(2,1)S(1)}, bf16[672,2048]{1,0:T(8,128)(2,1)}, u32[]{:S(2)}) copy-start(bf16[672,2048]{1,0:T(8,128)(2,1)} %param.11) | copy-start | bytes 8257540
  75.1 8.8 %copy-start.9 = (f32[2048]{0:T(1024)S(1)}, f32[2048]{0:T(1024)}, u32[]{:S(2)}) copy-start(f32[2048]{0:T(1024)} %param.8) | copy-start | bytes 24580
  83.9 7.8 %copy-start.11 = (f32[1536,672]{0,1:T(8,128)S(1)}, f32[1536,672]{0,1:T(8,128)}, u32[]{:S(2)}) copy-start(f32[1536,672]{0,1:T(8,128)} %fusion.5) | copy-start | bytes 12386308
  91.7 9.4 %copy-start.5 = (bf16[672,2048]{1,0:T(8,128)(2,1)S(1)}, bf16[672,2048]{1,0:T(8,128)(2,1)}, u32[]{:S(2)}) copy-start(bf16[672,2048]{1,0:T(8,128)(2,1)} %param.9) | copy-start | bytes 8257540
  101.2 1.5 copy-start.8
  101.2 1.9 %copy-start.6 = (bf16[1536,672]{0,1:T(8,128)(2,1)}, bf16[1536,672]{0,1:T(8,128)(2,1)S(1)}, u32[]{:S(2)}) copy-start(bf16[1536,672]{0,1:T(8,128)(2,1)S(1)} %get-tuple-element.11) | copy-start | bytes 6193156
  116.2 10.7 %copy-start.7 = (bf16[1536,672]{0,1:T(8,128)(2,1)S(1)}, bf16[1536,672]{0,1:T(8,128)(2,1)}, u32[]{:S(2)}) copy-start(bf16[1536,672]{0,1:T(8,128)(2,1)} %copy-done.6) | copy-start | bytes 6193156
  127.0 17.3 %copy-start.2 = (bf16[384,256]{1,0:T(8,128)(2,1)S(1)}, bf16[384,256]{1,0:T(8,128)(2,1)}, u32[]{:S(2)}) copy-start(bf16[384,256]{1,0:T(8,128)(2,1)} %x_ref.1) | copy-start | bytes 589828
  127.0 42.5 %copy-start.4 = (bf16[384,256]{1,0:T(8,128)(2,1)S(1)}, bf16[384,256]{1,0:T(8,128)(2,1)}, u32[]{:S(2)}) copy-start(bf16[384,256]{1,0:T(8,128)(2,1)} %dy_ref.1) | copy-start | bytes 589828
Sparse Core Ops, SparseCore 0:
  105.9 38.3 reduce-scatter.1
where the time goes:
time: 178 us
  Pallas kernels  61.6 us (35%)
  matrix products  61.1 us (34%)
  blocking collectives  24 us (13%)
  between operations  14.2 us (8%)
  waiting for transfers between devices  7.34 us (4%)
  other arithmetic  7.22 us (4%)
  local copies, waits for them, and re-layouts  2.68 us (2%)
    pallas_call x1, Pallas kernels, gather_all(): pl.pallas_call(functools.partial(gather_kernel, reps, tps), out_shape=jax...  61.6 us
    dot_general x3, matrix products, left_product(): lax.dot_general(left, right, (((0,), (0,)), ((), ())), preferred_element_...  31 us
    dot_general x3, matrix products, right_product(): lax.dot_general(left, weight, (((1,), (1,)), ((), ())), preferred_element...  26 us
    psum x2, blocking collectives, axis_sums(): return (lax.psum(rows_part, PLANE), lax.psum(gain_part, 'rep'))  24 us
    reduce_scatter x1, waiting for transfers between devices, input_grads(): lax.psum_scatter(partial_value, PLANE, scatter_dimension=1, tiled=True)  7.32 us
    reduce_sum x1, other arithmetic, normalise(): inv_rms = lax.rsqrt(jnp.mean(xf * xf, axis=1, keepdims=True) + EPS)  4.23 us
  transfers between devices with their start and end apart: 1, of which 1 were waited for; matrix products, arithmetic and copies ran while one was open for 17% of the time, Pallas kernels for 0%

commit v1 on v0

v1 whole, which is shorter than its diff:
```python
import functools

import jax
import jax.numpy as jnp
from jax import lax
from jax.experimental import pallas as pl
from jax.experimental.pallas import tpu as pltpu
from jax.sharding import PartitionSpec as P

EPS = 1e-06
PLANE = ("fs", "tp")


def right_product(left, weight):
    return lax.dot_general(
        left, weight, (((1,), (1,)), ((), ())), preferred_element_type=jnp.float32
    )


def left_product(left, right):
    return lax.dot_general(
        left, right, (((0,), (0,)), ((), ())), preferred_element_type=jnp.float32
    )


def normalise(x, gain):
    xf = x.astype(jnp.float32)
    inv_rms = lax.rsqrt(jnp.mean(xf * xf, axis=1, keepdims=True) + EPS)
    return inv_rms, (xf * inv_rms * gain).astype(jnp.bfloat16)


def hidden_grads(normed, dy, w_gate, w_up, w_down):
    gate = right_product(normed, w_gate)
    up = right_product(normed, w_up)
    sig = jax.nn.sigmoid(gate)
    active = gate * sig
    hidden = (active * up).astype(jnp.bfloat16)
    d_hidden = 0.5 * right_product(dy, w_down)
    d_gate = (d_hidden * up * sig * (1.0 + gate * (1.0 - sig))).astype(jnp.bfloat16)
    d_up = (d_hidden * active).astype(jnp.bfloat16)
    return hidden, d_gate, d_up


def hidden_sum(d_gate, d_up, w_gate, w_up):
    return jnp.dot(d_gate, w_gate, preferred_element_type=jnp.float32) + jnp.dot(
        d_up, w_up, preferred_element_type=jnp.float32
    )


def axis_sums(rows_part, gain_part):
    return lax.psum(rows_part, PLANE), lax.psum(gain_part, "rep")


def input_grads(tokens, cotangent, gain, inv_rms, partial_value, sums):
    width = partial_value.shape[1]
    summed = lax.psum_scatter(
        partial_value, PLANE, scatter_dimension=1, tiled=True
    ).astype(jnp.float32)
    own_width = summed.shape[1]
    unit_own = tokens.astype(jnp.float32) * inv_rms
    gain_own = lax.dynamic_slice_in_dim(
        gain, lax.axis_index(PLANE) * own_width, own_width, 0
    )
    d_unit = summed * gain_own
    row_sum, gain_part = sums(jnp.sum(unit_own * d_unit, axis=1), jnp.sum(unit_own * summed, axis=0))
    row_mean = row_sum / width
    grad_input = (
        cotangent.astype(jnp.float32) + inv_rms * (d_unit - unit_own * row_mean[:, None])
    ).astype(jnp.bfloat16)
    return grad_input, gain_part


def reduced(tokens, cotangent, gain, w_gate, w_up, w_down):
    full_x = lax.all_gather(tokens, PLANE, axis=1, tiled=True)
    full_dy = lax.all_gather(cotangent, PLANE, axis=1, tiled=True)
    inv_rms, normed = normalise(full_x, gain)
    hidden, d_gate, d_up = hidden_grads(normed, full_dy, w_gate, w_up, w_down)
    grad_down = 0.5 * left_product(hidden, full_dy)
    grad_gate = left_product(d_gate, normed)
    grad_up = left_product(d_up, normed)
    grad_input, gain_part = input_grads(
        tokens, cotangent, gain, inv_rms, hidden_sum(d_gate, d_up, w_gate, w_up),
        lambda rows_part, gain_part: (lax.psum(rows_part, PLANE), gain_part),
    )
    grad_gate, grad_up, grad_down, grad_gain = lax.psum(
        (grad_gate, grad_up, grad_down, gain_part), "rep"
    )
    return (grad_input, grad_gain, grad_gate, grad_up, grad_down)


TILE = 256
BLOCK = 64
MESH = pl.DeviceIdType.MESH
OWN, ACROSS_X, ACROSS_Y, CORNER = range(4)


def step_kernel(
    x_ref, dy_ref, gain_ref, wg_ref, wu_ref, wd_ref,
    grads, act, nrm, dy_tail, gi_ref, gg_ref,
    buf, wts, gain, inv, turned, pair_out, pair_in, own_sum, plane_out, plane_in,
    row_out, row_in, gain_out, gain_in,
    load_sem, send_sem, recv_sem, corner_sem, pair_sem,
    give_sem, take_sem, block_send, block_recv, row_send, row_recv, gain_send, gain_recv,
):
    z, y, t = lax.axis_index("rep"), lax.axis_index("fs"), lax.axis_index("tp")
    rows, cols = x_ref.shape
    hidden, width = wg_ref.shape
    total = 4 * rows
    half = rows // 2
    core = lax.rem(t, 2)
    other = 1 - 2 * core
    x_id = (z, y, lax.rem(t + 2, 4))
    y_id = (z, 1 - y, t)
    corner_id = (z, 1 - y, lax.rem(t + 2, 4))
    pair_id = (z, y, t + other)
    is_end = lax.rem(z + 1, 4) < 2
    is_mid = jnp.logical_not(is_end)
    inner_z = 1 + lax.rem(z, 2)
    inner_id = (inner_z, y, t)
    outer_id = (3 * lax.div(z, 2), y, t)
    inner_slot = 2 - lax.rem(lax.div(z + 1, 2), 2)
    column = (
        y * 4 + t,
        y * 4 + lax.rem(t + 2, 4),
        (1 - y) * 4 + t,
        (1 - y) * 4 + lax.rem(t + 2, 4),
    )
    pair_column = tuple(c + other for c in column)

    def across(col):
        return pl.ds(pl.multiple_of(col * cols, cols), cols)

    def piece(slot, col, p, start=0, size=rows):
        if isinstance(slot, int):
            window = pl.ds(slot * rows + start, size)
        else:
            window = pl.ds(pl.multiple_of(slot * rows + start, 64), size)
        return buf.at[p, window, across(col)]

    sent = []

    def send(make, guard=None):
        if guard is None:
            make().start()
        else:
            pl.when(guard)(lambda: make().start())
        sent.append((make, guard))

    def remote(src, dst, ssem, rsem, target):
        return pltpu.make_async_remote_copy(
            src_ref=src, dst_ref=dst, send_sem=ssem, recv_sem=rsem,
            device_id=target, device_id_type=MESH,
        )

    def arrive(ref, sem):
        pltpu.make_async_remote_copy(
            src_ref=ref, dst_ref=ref, send_sem=send_sem.at[0, 0, 0], recv_sem=sem,
            device_id=pair_id, device_id_type=MESH,
        ).wait_recv()

    def move(slot, q, p, kind, lands, target, start=0, size=rows):
        def make():
            ref = piece(slot, column[q], p, start, size)
            return remote(ref, ref, send_sem.at[kind, slot, p], lands[0].at[lands[1], slot, p], target)

        send(make)

    def to_pair(slot, q, p):
        move(slot, q, p, q, (pair_sem, q), pair_id)

    def to_x(slot, p):
        move(slot, OWN, p, 4, (recv_sem, ACROSS_X), x_id)

    def to_y(slot, p):
        move(slot, OWN, p, 5, (recv_sem, ACROSS_Y), y_id)

    def relay(slot, p):
        move(slot, ACROSS_X, p, 6, (corner_sem, 0), y_id, 0, half)
        move(slot, ACROSS_Y, p, 7, (corner_sem, 1), x_id, half, half)

    def along(slot, q, p, there, kind, target, guard):
        def make():
            return remote(
                piece(slot, column[q], p), piece(there, column[q], p),
                send_sem.at[kind, slot, p], recv_sem.at[q, there, p], target,
            )

        send(make, guard)

    def to_inner(slot, q, p, there, guard=None):
        along(slot, q, p, there, 8 if q == OWN else 9, inner_id, guard)

    def to_outer(slot, q, p, there):
        along(slot, q, p, there, 10 if q == OWN else 11, outer_id, is_mid)

    def landed(slot, q, p):
        arrive(piece(slot, column[q], p), recv_sem.at[q, slot, p])

    def corner_landed(slot, p):
        arrive(piece(slot, column[CORNER], p, 0, half), corner_sem.at[0, slot, p])
        arrive(piece(slot, column[CORNER], p, half, half), corner_sem.at[1, slot, p])

    def pair_landed(slot, p):
        for q in range(4):
            arrive(piece(slot, pair_column[q], p), pair_sem.at[q, slot, p])

    def own_piece(slot, p):
        landed(slot, OWN, p)
        if slot == 1:
            to_outer(1, OWN, p, 2)
        elif slot == 2:
            to_inner(2, OWN, p, 3, is_mid)
        else:
            to_outer(3, OWN, p, 3)
        to_pair(slot, OWN, p)

    def own_across(slot, p):
        to_x(slot, p)
        to_y(slot, p)

    def plane_piece(slot, p):
        landed(slot, ACROSS_X, p)
        landed(slot, ACROSS_Y, p)
        if slot in (0, 3):
            relay(slot, p)
        to_pair(slot, ACROSS_X, p)
        to_pair(slot, ACROSS_Y, p)

    def corner_piece(slot, p):
        if slot in (0, 3):
            corner_landed(slot, p)
        else:
            landed(slot, CORNER, p)
        if slot == 0:
            to_inner(0, CORNER, p, inner_slot)
            to_outer(0, CORNER, p, 1)
        elif slot == 1:
            to_outer(1, CORNER, p, 2)
        to_pair(slot, CORNER, p)

    def guarded(guard, act_on):
        before = len(sent)

        @pl.when(guard)
        def _():
            act_on()

        for i in range(before, len(sent)):
            make, inside = sent[i]
            sent[i] = (make, guard if inside is None else jnp.logical_and(guard, inside))

    loads = [
        pltpu.make_async_copy(ref, piece(0, column[OWN], p), load_sem.at[p])
        for p, ref in enumerate((x_ref, dy_ref))
    ]
    loads.append(pltpu.make_async_copy(gain_ref, gain, load_sem.at[2]))
    for i, ref in enumerate((wg_ref, wu_ref, wd_ref)):
        loads.append(pltpu.make_async_copy(ref, wts.at[i], load_sem.at[3 + i]))
    for load in loads:
        load.start()

    plane_peers = []
    for k in range(1, 8):
        far_y, far_x, far_core = k // 4, (k // 2) % 2, k % 2
        peer_t = lax.rem(t + 2 * far_x, 4)
        if far_core:
            peer_t = peer_t + other
        plane_peers.append((z, lax.rem(y + far_y, 2), peer_t))
    line_peers = [(lax.rem(z + k, 4), y, t) for k in range(1, 4)]
    barrier = pltpu.get_barrier_semaphore()
    for target in plane_peers + line_peers:
        pl.semaphore_signal(barrier, inc=1, device_id=target, device_id_type=MESH)
    pl.semaphore_wait(barrier, len(plane_peers) + len(line_peers))

    def normalise_rows(start, stop):
        gain_row = gain[...]

        def block(i, _):
            window = pl.ds(pl.multiple_of(start + i * BLOCK, BLOCK), BLOCK)
            xf = buf[0, window, :].astype(jnp.float32)
            scale = lax.rsqrt(jnp.sum(xf * xf, axis=1, keepdims=True) / width + EPS)
            nrm[window, :] = (xf * scale * gain_row).astype(jnp.bfloat16)
            if start == 0:
                inv[window, :] = jnp.broadcast_to(scale, (BLOCK, inv.shape[1]))
            return 0

        lax.fori_loop(0, (stop - start) // BLOCK, block, 0)

    def hidden_rows(start, stop, between=(lambda: None, lambda: None)):
        window = slice(start, stop)
        gate = right_product(wts[0], nrm[window, :])
        up = right_product(wts[1], nrm[window, :])
        between[0]()
        d_hidden = 0.5 * right_product(wts[2], buf[1, window, :])
        sig = jax.nn.sigmoid(gate)
        active = gate * sig
        act[0, :, window] = (active * up).astype(jnp.bfloat16)
        act[1, :, window] = (d_hidden * up * sig * (1.0 + gate * (1.0 - sig))).astype(jnp.bfloat16)
        act[2, :, window] = (d_hidden * active).astype(jnp.bfloat16)
        between[1]()

    def weight_grads(start, stop, first, last, fresh):
        window = slice(start, stop)
        step = 2 * TILE

        def tile(j, _):
            span = pl.ds(pl.multiple_of(j * step, step), step)
            for i, right in enumerate((nrm, nrm, None)):
                value = nrm[window, span] if right is not None else buf[1, window, span]
                left = act[(i + 1) % 3, :, window]
                product = jnp.dot(left, value, preferred_element_type=jnp.float32)
                if i == 2:
                    product = 0.5 * product
                if fresh:
                    grads[i, :, span] = product
                else:
                    grads[i, :, span] += product
            return 0

        lax.fori_loop(first * (width // step) // 4, last * (width // step) // 4, tile, 0)

    def feature_product(col):
        span = across(col)
        return jnp.dot(turned[0], wts[0, :, span], preferred_element_type=jnp.float32) + jnp.dot(
            turned[1], wts[1, :, span], preferred_element_type=jnp.float32
        )

    order = (CORNER, ACROSS_X, ACROSS_Y, OWN)
    block_ids = {CORNER: corner_id, ACROSS_X: x_id, ACROSS_Y: y_id}

    def give_pair():
        for i in range(2):
            turned[i] = act[1 + i, :, 0:rows].T
        for k, q in enumerate(order):
            pair_out[k] = feature_product(pair_column[q]).astype(jnp.bfloat16)
            send(lambda k=k: remote(pair_out.at[k], pair_in.at[k], give_sem.at[k], take_sem.at[k], pair_id))

    def give_plane():
        for k, q in enumerate(order):
            product = feature_product(column[q])
            arrive(pair_in.at[k], take_sem.at[k])
            product = product + pair_in[k].astype(jnp.float32)
            if q == OWN:
                own_sum[...] = product
            else:
                plane_out[k] = product.astype(jnp.bfloat16)
                send(lambda k=k, q=q: remote(
                    plane_out.at[k], plane_in.at[k], block_send.at[k], block_recv.at[k], block_ids[q]
                ))

    def own_values():
        unit = buf[0, 0:rows, across(column[OWN])].astype(jnp.float32) * inv[:, 0:1]
        gain_own = gain[0:1, across(column[OWN])]
        return unit, gain_own

    def take_plane():
        for k in range(3):
            arrive(plane_in.at[k], block_recv.at[k])
        summed = own_sum[...]
        for k in range(3):
            summed = summed + plane_in[k].astype(jnp.float32)
        own_sum[...] = summed
        unit, gain_own = own_values()
        product = unit * summed
        gain_out[...] = jnp.broadcast_to(jnp.sum(product, axis=0, keepdims=True), gain_out.shape)
        product = product * gain_own
        lanes = inv.shape[1]
        folded = product[:, 0:lanes]
        for i in range(1, cols // lanes):
            folded = folded + product[:, i * lanes:(i + 1) * lanes]
        row_out[...] = jnp.broadcast_to(jnp.sum(folded.T, axis=0, keepdims=True), row_out.shape)
        for k, target in enumerate(plane_peers):
            send(lambda k=k, target=target: remote(
                row_out, row_in.at[k], row_send.at[k], row_recv.at[k], target
            ))
        for k, target in enumerate(line_peers):
            send(lambda k=k, target=target: remote(
                gain_out, gain_in.at[k], gain_send.at[k], gain_recv.at[k], target
            ))

    def finish_input():
        row = row_out[0:1, :]
        for k in range(7):
            arrive(row_in.at[k], row_recv.at[k])
            row = row + row_in[k, 0:1, :]
        summed_gain = gain_out[...]
        for k in range(3):
            arrive(gain_in.at[k], gain_recv.at[k])
            summed_gain = summed_gain + gain_in[k]
        gg_ref[...] = summed_gain
        lanes = inv.shape[1]
        row_mean = jnp.broadcast_to(row / width, (lanes, rows)).T
        unit, gain_own = own_values()
        d_unit = own_sum[...] * gain_own
        dy_own = buf[1, 0:rows, across(column[OWN])].astype(jnp.float32)
        gi_ref[...] = (dy_own + inv[:, 0:1] * (d_unit - unit * row_mean[:, 0:1])).astype(gi_ref.dtype)

    for p in range(2):
        loads[p].wait()
        to_inner(0, OWN, p, inner_slot)
        to_outer(0, OWN, p, 1)
        to_x(0, p)
        to_y(0, p)
        to_pair(0, OWN, p)
    for p in range(2):
        plane_piece(0, p)
        own_piece(1, p)
        guarded(is_mid, lambda: own_piece(2, p))
    own_across(1, 0)
    own_across(1, 1)

    def middle_across():
        own_across(2, 0)
        own_across(2, 1)

    guarded(is_mid, middle_across)
    corner_piece(0, 0)
    corner_piece(0, 1)
    loads[2].wait()
    pair_landed(0, 0)
    normalise_rows(0, rows)

    def later(p):
        def at_end():
            own_piece(2, p)
            own_across(2, p)

        def at_middle():
            own_piece(3, p)
            own_across(3, p)

        guarded(is_end, at_end)
        guarded(is_mid, at_middle)

    later(0)
    for i in range(3):
        loads[3 + i].wait()
    pair_landed(0, 1)
    hidden_rows(0, rows, (lambda: later(1), lambda: plane_piece(1, 0)))
    give_pair()
    plane_piece(1, 1)
    give_plane()
    corner_piece(1, 0)
    corner_piece(1, 1)
    pair_landed(1, 0)
    pair_landed(1, 1)
    middle = (rows + TILE, rows + 2 * TILE, rows + 3 * TILE)
    normalise_rows(rows, middle[0])
    hidden_rows(rows, middle[0], (lambda: plane_piece(2, 0), lambda: plane_piece(2, 1)))
    split = total // 3

    def end_across(p):
        def act_on():
            own_piece(3, p)
            own_across(3, p)

        guarded(is_end, act_on)

    weight_grads(0, split, 0, 2, True)
    end_across(0)
    weight_grads(0, split, 2, 4, True)
    end_across(1)
    take_plane()
    corner_piece(2, 0)
    corner_piece(2, 1)
    pair_landed(2, 0)
    pair_landed(2, 1)
    normalise_rows(middle[0], middle[1])
    hidden_rows(middle[0], middle[1])
    finish_input()
    normalise_rows(middle[1], middle[2])
    hidden_rows(middle[1], middle[2])
    plane_piece(3, 0)
    weight_grads(split, 2 * split, 0, 2, False)
    plane_piece(3, 1)
    weight_grads(split, 2 * split, 2, 4, False)
    corner_piece(3, 0)
    pair_landed(3, 0)
    normalise_rows(3 * rows, total)

    def rest():
        corner_piece(3, 1)
        pair_landed(3, 1)

    hidden_rows(3 * rows, total, (rest, lambda: None))
    dy_tail[...] = buf[1, 2 * split:, :]
    for make, guard in sent:
        if guard is None:
            make().wait_send()
        else:
            pl.when(guard)(lambda make=make: make().wait_send())


def fused_step(tokens, cotangent, gain, w_gate, w_up, w_down):
    rows, cols = tokens.shape
    hidden, width = w_gate.shape
    total = 4 * rows
    half_type, full_type = jnp.bfloat16, jnp.float32
    hbm = pl.BlockSpec(memory_space=pltpu.HBM)
    vmem = pl.BlockSpec(memory_space=pltpu.VMEM)
    dma = pltpu.SemaphoreType.DMA
    return pl.pallas_call(
        step_kernel,
        out_shape=[
            pltpu.VMEM((3, hidden, width), full_type),
            pltpu.VMEM((3, hidden, total), half_type),
            pltpu.VMEM((total, width), half_type),
            pltpu.VMEM((total // 3, width), half_type),
            pltpu.VMEM((rows, cols), half_type),
            pltpu.VMEM((8, cols), full_type),
        ],
        in_specs=[hbm] * 6,
        out_specs=[vmem] * 6,
        scratch_shapes=[
            pltpu.VMEM((2, total, width), half_type),
            pltpu.VMEM((3, hidden, width), half_type),
            pltpu.VMEM((1, width), full_type),
            pltpu.VMEM((rows, 128), full_type),
            pltpu.VMEM((2, rows, hidden), half_type),
            pltpu.VMEM((4, rows, cols), half_type),
            pltpu.VMEM((4, rows, cols), half_type),
            pltpu.VMEM((rows, cols), full_type),
            pltpu.VMEM((3, rows, cols), half_type),
            pltpu.VMEM((3, rows, cols), half_type),
            pltpu.VMEM((8, rows), full_type),
            pltpu.VMEM((7, 8, rows), full_type),
            pltpu.VMEM((8, cols), full_type),
            pltpu.VMEM((3, 8, cols), full_type),
            dma((6,)), dma((12, 4, 2)), dma((4, 4, 2)), dma((2, 4, 2)), dma((4, 4, 2)),
            dma((4,)), dma((4,)), dma((3,)), dma((3,)), dma((7,)), dma((7,)), dma((3,)), dma((3,)),
        ],
        compiler_params=pltpu.CompilerParams(
            collective_id=0, has_side_effects=True, vmem_limit_bytes=30 * 2**20
        ),
        name="step",
    )(tokens, cotangent, gain.reshape(1, width), w_gate, w_up, w_down)


def last_kernel(grads, act, nrm, dy, gi, gg, gate_ref, up_ref, down_ref, gi_ref, gg_ref, stage, sem):
    width = nrm.shape[1]
    count = dy.shape[0]
    start = nrm.shape[0] - count
    step = 2 * TILE
    outs = (gate_ref, up_ref, down_ref)
    small = [
        pltpu.make_async_copy(gi, gi_ref, sem.at[2, 0]),
        pltpu.make_async_copy(gg, gg_ref, sem.at[2, 1]),
    ]
    for copy in small:
        copy.start()
    waiting = [[], []]
    for j in range(width // step):
        span = slice(j * step, (j + 1) * step)
        slot = j % 2
        for copy in waiting[slot]:
            copy.wait()
        waiting[slot] = []
        for i in range(3):
            left = act[(i + 1) % 3, :, start:]
            value = dy[:, span] if i == 2 else nrm[start:, span]
            product = jnp.dot(left, value, preferred_element_type=jnp.float32)
            if i == 2:
                product = 0.5 * product
            stage[slot, i] = grads[i, :, span] + product
            copy = pltpu.make_async_copy(stage.at[slot, i], outs[i].at[:, span], sem.at[slot, i])
            copy.start()
            waiting[slot].append(copy)
    for copy in waiting[0] + waiting[1] + small:
        copy.wait()


def fused(tokens, cotangent, gain, w_gate, w_up, w_down):
    rows, cols = tokens.shape
    hidden, width = w_gate.shape
    parts = fused_step(tokens, cotangent, gain, w_gate, w_up, w_down)
    full = jax.ShapeDtypeStruct((hidden, width), jnp.float32)
    vmem = pl.BlockSpec(memory_space=pltpu.VMEM)
    grad_gate, grad_up, grad_down, grad_input, grad_gain = pl.pallas_call(
        last_kernel,
        out_shape=[
            full, full, full,
            jax.ShapeDtypeStruct((rows, cols), tokens.dtype),
            jax.ShapeDtypeStruct((8, cols), jnp.float32),
        ],
        in_specs=[vmem] * 6,
        out_specs=[pl.BlockSpec(memory_space=pltpu.HBM)] * 5,
        scratch_shapes=[
            pltpu.VMEM((2, 3, hidden, 2 * TILE), jnp.float32),
            pltpu.SemaphoreType.DMA((3, 3)),
        ],
        compiler_params=pltpu.CompilerParams(vmem_limit_bytes=20 * 2**20),
        name="last",
    )(*parts)
    return grad_input, grad_gain[0], grad_gate, grad_up, grad_down


def fits_fused(tokens, w_gate):
    sizes = tuple(lax.axis_size(name) for name in ("rep", "fs", "tp"))
    rows, cols = tokens.shape
    hidden, width = w_gate.shape
    return (
        sizes == (4, 2, 4)
        and rows == TILE + TILE // 2
        and cols == TILE
        and width == 8 * cols
        and hidden % 16 == 0
        and 24 * hidden * width <= 34 * 2**20
    )


def gathered(tokens, cotangent, gain, w_gate, w_up, w_down):
    rows, cols = tokens.shape
    reps, plane = lax.axis_size("rep"), lax.axis_size(PLANE)
    both = lax.all_gather(jnp.stack([tokens, cotangent]), ("rep",) + PLANE)
    both = both.reshape(reps, plane, 2, rows, cols).transpose(2, 0, 3, 1, 4)
    both = both.reshape(2, reps * rows, plane * cols)
    inv_rms, normed = normalise(both[0], gain)
    dy = both[1]
    hidden, d_gate, d_up = hidden_grads(normed, dy, w_gate, w_up, w_down)
    start = lax.axis_index("rep") * rows
    own = lambda a: lax.dynamic_slice_in_dim(a, start, rows, 0)
    partial_value = hidden_sum(own(d_gate), own(d_up), w_gate, w_up).astype(jnp.bfloat16)
    partial_value, hidden, d_gate, d_up = lax.optimization_barrier(
        (partial_value, hidden, d_gate, d_up)
    )
    grad_input, grad_gain = input_grads(
        tokens, cotangent, gain, own(inv_rms), partial_value, axis_sums
    )
    grad_down = 0.5 * left_product(hidden, dy)
    grad_gate = left_product(d_gate, normed)
    grad_up = left_product(d_up, normed)
    return (grad_input, grad_gain, grad_gate, grad_up, grad_down)


def local(tokens, cotangent, gain, w_gate, w_up, w_down):
    reps = lax.axis_size("rep")
    token_bytes = 2 * 2 * tokens.shape[0] * reps * w_gate.shape[1]
    grad_bytes = 3 * 4 * w_gate.size
    plan = gathered if token_bytes < grad_bytes else reduced
    if fits_fused(tokens, w_gate):
        plan = fused
    return plan(tokens, cotangent, gain, w_gate, w_up, w_down)


def solution(mesh):
    placed = (
        P("rep", PLANE),
        P("rep", PLANE),
        P(),
        P(PLANE, None),
        P(PLANE, None),
        P(PLANE, None),
    )
    return jax.shard_map(
        local,
        mesh=mesh,
        in_specs=placed,
        out_specs=(
            P("rep", PLANE),
            P(PLANE),
            P(PLANE, None),
            P(PLANE, None),
            P(PLANE, None),
        ),
        check_vma=False,
    )
```

time: 178 us -> 101 us (0.57)
  matrix products: 61.1 us -> 0 us
  blocking collectives: 24 us -> 0 us
  Pallas kernels: 61.6 us -> 82.2 us
  local copies, waits for them, and re-layouts: 2.68 us -> 17.3 us
  between operations: 14.2 us -> 0.66 us
  waiting for transfers between devices: 7.34 us -> 0 us
  other arithmetic: 7.22 us -> 0 us
    dot_general x8 -> x0, matrix products: 61.1 us -> none  [the longest x3 31 us: left_product(): lax.dot_general(left, right, (((0,), (0,)), ((), ())), preferred_element_...]
    psum x2 -> x0, blocking collectives: 24 us -> none  [axis_sums(): return (lax.psum(rows_part, PLANE), lax.psum(gain_part, 'rep'))]
    pallas_call x1 -> x2, Pallas kernels: 61.6 us -> 82.2 us  [the longest x1 75.9 us: fused_step(): pl.pallas_call(step_kernel, out_shape=[pltpu.VMEM((3, hidden, width), ful...]
    unnamed x24 -> x8, local copies, waits for them, and re-layouts: 2.53 us -> 16.7 us
    reduce_scatter x1 -> x0, waiting for transfers between devices: 7.32 us -> none  [input_grads(): lax.psum_scatter(partial_value, PLANE, scatter_dimension=1, tiled=True)]
    reduce_sum x2 -> x0, other arithmetic: 5.4 us -> none  [the longest x1 4.23 us: normalise(): inv_rms = lax.rsqrt(jnp.mean(xf * xf, axis=1, keepdims=True) + EPS)]
    convert_element_type x1 -> x0, other arithmetic: 1.81 us -> none  [input_grads(): grad_input = (cotangent.astype(jnp.float32) + inv_rms * (d_unit - unit_ow...]
  transfers between devices with their start and end apart: 1 -> 0, of which waited for: 1 -> 0; matrix products, arithmetic and copies ran while one was open for 17% -> 0% of each run, Pallas kernels for 0% -> 0%
where the time goes in v1:
time: 101 us; the launch traced here: 100 us
  Pallas kernels  82.2 us (81%)
  local copies, waits for them, and re-layouts  17.3 us (17%)
    pallas_call x1, Pallas kernels, fused_step(): pl.pallas_call(step_kernel, out_shape=[pltpu.VMEM((3, hidden, width), ful...  75.9 us
    unnamed x8, local copies, waits for them, and re-layouts  16.7 us
    pallas_call x1, Pallas kernels, fused(): pl.pallas_call(last_kernel, out_shape=[full, full, full, jax.ShapeDtypeSt...  6.36 us

profile of v1, /device:TPU:0, one launch (start us, length us, event | category | flops | bytes accessed | tf_op | source)
XLA Modules:
  0.0 100.2 jit_solution(395662090195504818)
XLA Ops:
  0.6 75.9 %step.1 = (f32[3,672,2048]{2,1,0:T(8,128)S(1)}, bf16[3,672,1536]{2,1,0:T(8,128)(2,1)S(1)}, bf16[1536,2048]{1,0:T(8,128)(2,1)S(1)}, bf16[512,2048]{1,0:T(8,128)(2...) custom-call(bf16[384,256]{1,0:T(8,128)(2,1)} %x_ref.1, bf16[384,256]{1,0:T(8,128)(2,1)} %dy_ref.1, ...), custom_call_target="tpu_custom_call" | custom-call | tf_op jit(solution)/shard_map/step/pallas_call | solution.py:502
  76.5 0.0 copy-start
  76.5 5.7 %copy-done = f32[3,672,2048]{2,1,0:T(8,128)} copy-done((f32[3,672,2048]{2,1,0:T(8,128)}, f32[3,672,2048]{2,1,0:T(8,128)S(1)}, u32[]{:S(2)}) %copy-start) | copy-done | bytes 16515096
  82.2 0.0 copy-start.2
  82.2 2.6 %copy-done.2 = bf16[3,672,1536]{2,1,0:T(8,128)(2,1)} copy-done((bf16[3,672,1536]{2,1,0:T(8,128)(2,1)}, bf16[3,672,1536]{2,1,0:T(8,128)(2,1)S(1)}, u32[]{:S(2)}) %copy-start.2) | copy-done | bytes 6193176
  84.8 0.0 copy-start.1
  84.8 5.7 %copy-done.1 = f32[3,672,2048]{2,1,0:T(8,128)S(1)} copy-done((f32[3,672,2048]{2,1,0:T(8,128)S(1)}, f32[3,672,2048]{2,1,0:T(8,128)}, u32[]{:S(2)}) %copy-start.1) | copy-done | bytes 16515096
  90.5 0.0 copy-start.3
  90.5 2.8 %copy-done.3 = bf16[3,672,1536]{2,1,0:T(8,128)(2,1)S(1)} copy-done((bf16[3,672,1536]{2,1,0:T(8,128)(2,1)S(1)}, bf16[3,672,1536]{2,1,0:T(8,128)(2,1)}, u32[]{:S(2)}) %copy-start.3) | copy-done | bytes 6193176
  93.3 6.4 %last.1 = (f32[672,2048]{1,0:T(8,128)}, f32[672,2048]{1,0:T(8,128)}, f32[672,2048]{1,0:T(8,128)}, bf16[384,256]{1,0:T(8,128)(2,1)}, f32[8,256]{1,0:T(8,128)S(1)}) custom-call(f32[3,672,2048]{2,1,0:T(8,128)S(1)} %copy-done.1, bf16[3,672,1536]{2,1,0:T(8,128)(2,1)S(1)} %copy-done.3, bf16[1536,2048]{1,0:T(8,128)(2,1)S(1)} %get-tuple-element.18.nrm, ...), custom_call_target="tpu_custom_call" | custom-call | tf_op jit(solution)/shard_map/last/pallas_call | solution.py:578
  99.6 0.6 slice.3
Async XLA Ops:
  76.5 5.7 %copy-start = (f32[3,672,2048]{2,1,0:T(8,128)}, f32[3,672,2048]{2,1,0:T(8,128)S(1)}, u32[]{:S(2)}) copy-start(f32[3,672,2048]{2,1,0:T(8,128)S(1)} %get-tuple-element.16.grads) | copy-start | bytes 49545220
  82.2 2.6 %copy-start.2 = (bf16[3,672,1536]{2,1,0:T(8,128)(2,1)}, bf16[3,672,1536]{2,1,0:T(8,128)(2,1)S(1)}, u32[]{:S(2)}) copy-start(bf16[3,672,1536]{2,1,0:T(8,128)(2,1)S(1)} %get-tuple-element.17.act) | copy-start | bytes 18579460
  84.8 5.7 %copy-start.1 = (f32[3,672,2048]{2,1,0:T(8,128)S(1)}, f32[3,672,2048]{2,1,0:T(8,128)}, u32[]{:S(2)}) copy-start(f32[3,672,2048]{2,1,0:T(8,128)} %copy-done) | copy-start | bytes 49545220
  90.5 2.8 %copy-start.3 = (bf16[3,672,1536]{2,1,0:T(8,128)(2,1)S(1)}, bf16[3,672,1536]{2,1,0:T(8,128)(2,1)}, u32[]{:S(2)}) copy-start(bf16[3,672,1536]{2,1,0:T(8,128)(2,1)} %copy-done.2) | copy-start | bytes 18579460

commit v2 on v1

--- a/solution.py
+++ b/solution.py
@@ -96,10 +96,10 @@
 
 def step_kernel(
     x_ref, dy_ref, gain_ref, wg_ref, wu_ref, wd_ref,
-    grads, act, nrm, dy_tail, gi_ref, gg_ref,
-    buf, wts, gain, inv, turned, pair_out, pair_in, own_sum, plane_out, plane_in,
+    grad_a, grad_b, grad_c, act_tail, nrm_tail, dy_tail, gi_ref, gg_ref,
+    act_main, nrm_main, buf, wts, gain, inv, turned, own_part, pair_out, pair_in, own_sum, plane_out, plane_in,
     row_out, row_in, gain_out, gain_in,
-    load_sem, send_sem, recv_sem, corner_sem, pair_sem,
+    load_sem, send_sem, recv_sem, corner_sem, pair_sem, late_sem,
     give_sem, take_sem, block_send, block_recv, row_send, row_recv, gain_send, gain_recv,
 ):
     z, y, t = lax.axis_index("rep"), lax.axis_index("fs"), lax.axis_index("tp")
@@ -107,6 +107,7 @@
     hidden, width = wg_ref.shape
     total = 4 * rows
     half = rows // 2
+    split = rows + TILE
     core = lax.rem(t, 2)
     other = 1 - 2 * core
     x_id = (z, y, lax.rem(t + 2, 4))
@@ -137,6 +138,7 @@
             window = pl.ds(pl.multiple_of(slot * rows + start, 64), size)
         return buf.at[p, window, across(col)]
 
+    grads = (grad_a, grad_b, grad_c)
     sent = []
 
     def send(make, guard=None):
@@ -144,7 +146,7 @@
             make().start()
         else:
             pl.when(guard)(lambda: make().start())
-        sent.append((make, guard))
+        sent.append((make, () if guard is None else (guard,)))
 
     def remote(src, dst, ssem, rsem, target):
         return pltpu.make_async_remote_copy(
@@ -173,6 +175,15 @@
 
     def to_y(slot, p):
         move(slot, OWN, p, 5, (recv_sem, ACROSS_Y), y_id)
+
+    def split_across(p, first):
+        a, b = (0, half) if first else (half, 0)
+        if first:
+            move(0, OWN, p, 4, (recv_sem, ACROSS_X), x_id, a, half)
+            move(0, OWN, p, 5, (recv_sem, ACROSS_Y), y_id, b, half)
+        else:
+            move(0, OWN, p, 12, (late_sem, 0), x_id, a, half)
+            move(0, OWN, p, 13, (late_sem, 1), y_id, b, half)
 
     def relay(slot, p):
         move(slot, ACROSS_X, p, 6, (corner_sem, 0), y_id, 0, half)
@@ -204,38 +215,59 @@
         for q in range(4):
             arrive(piece(slot, pair_column[q], p), pair_sem.at[q, slot, p])
 
+    def onward(slot, q, p):
+        if slot == 1:
+            to_outer(1, q, p, 2)
+        elif slot == 2:
+            to_inner(2, q, p, 3, is_mid)
+        else:
+            to_outer(3, q, p, 3)
+
     def own_piece(slot, p):
         landed(slot, OWN, p)
-        if slot == 1:
-            to_outer(1, OWN, p, 2)
-        elif slot == 2:
-            to_inner(2, OWN, p, 3, is_mid)
-        else:
-            to_outer(3, OWN, p, 3)
+        onward(slot, OWN, p)
         to_pair(slot, OWN, p)
 
     def own_across(slot, p):
         to_x(slot, p)
         to_y(slot, p)
 
+    def split_landed(p):
+        arrive(piece(0, column[ACROSS_X], p, 0, half), recv_sem.at[ACROSS_X, 0, p])
+        arrive(piece(0, column[ACROSS_Y], p, half, half), recv_sem.at[ACROSS_Y, 0, p])
+        relay(0, p)
+
+    def split_rest(p):
+        arrive(piece(0, column[ACROSS_X], p, half, half), late_sem.at[0, 0, p])
+        arrive(piece(0, column[ACROSS_Y], p, 0, half), late_sem.at[1, 0, p])
+        to_pair(0, ACROSS_X, p)
+        to_pair(0, ACROSS_Y, p)
+
     def plane_piece(slot, p):
         landed(slot, ACROSS_X, p)
         landed(slot, ACROSS_Y, p)
-        if slot in (0, 3):
-            relay(slot, p)
+        if slot == 0:
+            relay(0, p)
+        elif slot == 1:
+            guarded(is_end, lambda: relay(1, p))
         to_pair(slot, ACROSS_X, p)
         to_pair(slot, ACROSS_Y, p)
 
     def corner_piece(slot, p):
-        if slot in (0, 3):
-            corner_landed(slot, p)
+        if slot == 0:
+            corner_landed(0, p)
+            to_inner(0, CORNER, p, inner_slot)
+        elif slot == 1:
+            pl.when(is_end)(lambda: corner_landed(1, p))
+
+            def passed_on():
+                landed(1, CORNER, p)
+                onward(1, CORNER, p)
+
+            guarded(is_mid, passed_on)
         else:
             landed(slot, CORNER, p)
-        if slot == 0:
-            to_inner(0, CORNER, p, inner_slot)
-            to_outer(0, CORNER, p, 1)
-        elif slot == 1:
-            to_outer(1, CORNER, p, 2)
+            onward(slot, CORNER, p)
         to_pair(slot, CORNER, p)
 
     def guarded(guard, act_on):
@@ -247,7 +279,7 @@
 
         for i in range(before, len(sent)):
             make, inside = sent[i]
-            sent[i] = (make, guard if inside is None else jnp.logical_and(guard, inside))
+            sent[i] = (make, (guard,) + inside)
 
     loads = [
         pltpu.make_async_copy(ref, piece(0, column[OWN], p), load_sem.at[p])
@@ -272,81 +304,103 @@
         pl.semaphore_signal(barrier, inc=1, device_id=target, device_id_type=MESH)
     pl.semaphore_wait(barrier, len(plane_peers) + len(line_peers))
 
+    def place(start):
+        if start < 3 * rows:
+            return act_main, nrm_main, start if start < split else start - split
+        return act_tail, nrm_tail, start - 3 * rows
+
     def normalise_rows(start, stop):
         gain_row = gain[...]
+        _, nrm, base = place(start)
 
         def block(i, _):
             window = pl.ds(pl.multiple_of(start + i * BLOCK, BLOCK), BLOCK)
             xf = buf[0, window, :].astype(jnp.float32)
             scale = lax.rsqrt(jnp.sum(xf * xf, axis=1, keepdims=True) / width + EPS)
-            nrm[window, :] = (xf * scale * gain_row).astype(jnp.bfloat16)
+            nrm[pl.ds(pl.multiple_of(base + i * BLOCK, BLOCK), BLOCK), :] = (
+                xf * scale * gain_row
+            ).astype(jnp.bfloat16)
             if start == 0:
                 inv[window, :] = jnp.broadcast_to(scale, (BLOCK, inv.shape[1]))
             return 0
 
-        lax.fori_loop(0, (stop - start) // BLOCK, block, 0)
-
-    def hidden_rows(start, stop, between=(lambda: None, lambda: None)):
-        window = slice(start, stop)
+        lax.fori_loop(0, (stop - start) // BLOCK, block, 0, unroll=2)
+
+    def hidden_rows(start, stop, hooks=()):
+        hooks = hooks + (lambda: None,) * (4 - len(hooks))
+        last = start == 3 * rows
+        act, nrm, base = place(start)
+        window = slice(base, base + stop - start)
         gate = right_product(wts[0], nrm[window, :])
+        hooks[0]()
         up = right_product(wts[1], nrm[window, :])
-        between[0]()
-        d_hidden = 0.5 * right_product(wts[2], buf[1, window, :])
+        hooks[1]()
+        if last:
+            dy_tail[...] = buf[1, start:stop, :]
+        d_hidden = 0.5 * right_product(wts[2], buf[1, start:stop, :])
+        hooks[2]()
         sig = jax.nn.sigmoid(gate)
         active = gate * sig
         act[0, :, window] = (active * up).astype(jnp.bfloat16)
         act[1, :, window] = (d_hidden * up * sig * (1.0 + gate * (1.0 - sig))).astype(jnp.bfloat16)
         act[2, :, window] = (d_hidden * active).astype(jnp.bfloat16)
-        between[1]()
+        hooks[3]()
 
     def weight_grads(start, stop, first, last, fresh):
-        window = slice(start, stop)
-        step = 2 * TILE
+        act, nrm, base = place(start)
+        window = slice(base, base + stop - start)
+        step = 4 * TILE if stop - start == TILE else 2 * TILE
 
         def tile(j, _):
             span = pl.ds(pl.multiple_of(j * step, step), step)
             for i, right in enumerate((nrm, nrm, None)):
-                value = nrm[window, span] if right is not None else buf[1, window, span]
+                value = nrm[window, span] if right is not None else buf[1, start:stop, span]
                 left = act[(i + 1) % 3, :, window]
                 product = jnp.dot(left, value, preferred_element_type=jnp.float32)
                 if i == 2:
                     product = 0.5 * product
                 if fresh:
-                    grads[i, :, span] = product
+                    grads[i][:, span] = product
                 else:
-                    grads[i, :, span] += product
+                    grads[i][:, span] += product
             return 0
 
         lax.fori_loop(first * (width // step) // 4, last * (width // step) // 4, tile, 0)
 
-    def feature_product(col):
-        span = across(col)
-        return jnp.dot(turned[0], wts[0, :, span], preferred_element_type=jnp.float32) + jnp.dot(
-            turned[1], wts[1, :, span], preferred_element_type=jnp.float32
-        )
-
-    order = (CORNER, ACROSS_X, ACROSS_Y, OWN)
+    order = (ACROSS_X, ACROSS_Y, CORNER, OWN)
     block_ids = {CORNER: corner_id, ACROSS_X: x_id, ACROSS_Y: y_id}
 
     def give_pair():
         for i in range(2):
-            turned[i] = act[1 + i, :, 0:rows].T
+            turned[i] = act_main[1 + i, :, 0:rows].T
         for k, q in enumerate(order):
-            pair_out[k] = feature_product(pair_column[q]).astype(jnp.bfloat16)
+            both = pl.ds(pl.multiple_of((column[q] - core) * cols, 2 * cols), 2 * cols)
+            product = jnp.dot(turned[0], wts[0, :, both], preferred_element_type=jnp.float32) + jnp.dot(
+                turned[1], wts[1, :, both], preferred_element_type=jnp.float32
+            )
+
+            def keep(mine, theirs, k=k):
+                own_part[k] = mine
+                pair_out[k] = theirs.astype(jnp.bfloat16)
+
+            low, high = product[:, :cols], product[:, cols:]
+            pl.when(core == 0)(lambda: keep(low, high))
+            pl.when(core == 1)(lambda: keep(high, low))
             send(lambda k=k: remote(pair_out.at[k], pair_in.at[k], give_sem.at[k], take_sem.at[k], pair_id))
 
     def give_plane():
         for k, q in enumerate(order):
-            product = feature_product(column[q])
             arrive(pair_in.at[k], take_sem.at[k])
-            product = product + pair_in[k].astype(jnp.float32)
+            product = own_part[k] + pair_in[k].astype(jnp.float32)
             if q == OWN:
                 own_sum[...] = product
             else:
                 plane_out[k] = product.astype(jnp.bfloat16)
-                send(lambda k=k, q=q: remote(
-                    plane_out.at[k], plane_in.at[k], block_send.at[k], block_recv.at[k], block_ids[q]
-                ))
+
+    def send_plane(k):
+        send(lambda: remote(
+            plane_out.at[k], plane_in.at[k], block_send.at[k], block_recv.at[k], block_ids[order[k]]
+        ))
 
     def own_values():
         unit = buf[0, 0:rows, across(column[OWN])].astype(jnp.float32) * inv[:, 0:1]
@@ -387,7 +441,7 @@
         for k in range(3):
             arrive(gain_in.at[k], gain_recv.at[k])
             summed_gain = summed_gain + gain_in[k]
-        gg_ref[...] = summed_gain
+        gg_ref[...] = summed_gain[0:1, :]
         lanes = inv.shape[1]
         row_mean = jnp.broadcast_to(row / width, (lanes, rows)).T
         unit, gain_own = own_values()
@@ -399,13 +453,20 @@
         loads[p].wait()
         to_inner(0, OWN, p, inner_slot)
         to_outer(0, OWN, p, 1)
-        to_x(0, p)
-        to_y(0, p)
+        if p == 0:
+            to_x(0, p)
+            to_y(0, p)
+        else:
+            split_across(p, True)
         to_pair(0, OWN, p)
-    for p in range(2):
-        plane_piece(0, p)
-        own_piece(1, p)
-        guarded(is_mid, lambda: own_piece(2, p))
+    plane_piece(0, 0)
+    split_across(1, False)
+    own_piece(1, 0)
+    guarded(is_mid, lambda: own_piece(2, 0))
+    split_landed(1)
+    own_piece(1, 1)
+    guarded(is_mid, lambda: own_piece(2, 1))
+    corner_piece(0, 0)
     own_across(1, 0)
     own_across(1, 1)
 
@@ -414,81 +475,95 @@
         own_across(2, 1)
 
     guarded(is_mid, middle_across)
-    corner_piece(0, 0)
-    corner_piece(0, 1)
+
+    def either(at_end, at_mid):
+        guarded(is_end, at_end)
+        guarded(is_mid, at_mid)
+
+    def all_of(*steps):
+        def run():
+            for step in steps:
+                step()
+
+        return run
+
+    def far_own(p):
+        either(lambda: own_piece(2, p), lambda: own_piece(3, p))
+
+    def end_across():
+        for p in range(2):
+            guarded(is_end, lambda: own_across(2, p))
+
+    def last_own(p):
+        either(lambda: own_piece(3, p), lambda: corner_piece(1, p))
+
+    def mid_corner(slot, p):
+        guarded(is_mid, lambda: corner_piece(slot, p))
+
+    def end_corner(slot, p):
+        guarded(is_end, lambda: corner_piece(slot, p))
+
     loads[2].wait()
     pair_landed(0, 0)
     normalise_rows(0, rows)
-
-    def later(p):
-        def at_end():
-            own_piece(2, p)
-            own_across(2, p)
-
-        def at_middle():
-            own_piece(3, p)
-            own_across(3, p)
-
-        guarded(is_end, at_end)
-        guarded(is_mid, at_middle)
-
-    later(0)
+    split_rest(1)
     for i in range(3):
         loads[3 + i].wait()
-    pair_landed(0, 1)
-    hidden_rows(0, rows, (lambda: later(1), lambda: plane_piece(1, 0)))
+    hidden_rows(0, rows, (
+        all_of(lambda: corner_piece(0, 1), lambda: far_own(0)),
+        lambda: pair_landed(0, 1),
+        lambda: mid_corner(2, 0),
+        all_of(lambda: plane_piece(1, 0), lambda: far_own(1)),
+    ))
     give_pair()
+    mid_corner(2, 1)
+    weight_grads(0, rows, 0, 1, True)
     plane_piece(1, 1)
+    end_across()
+    last_own(0)
     give_plane()
-    corner_piece(1, 0)
-    corner_piece(1, 1)
-    pair_landed(1, 0)
-    pair_landed(1, 1)
+    end_corner(1, 0)
+    weight_grads(0, rows, 1, 3, True)
+    last_own(1)
+    end_corner(1, 1)
+    weight_grads(0, rows, 3, 4, True)
+    send_plane(0)
+    send_plane(1)
+    for p in range(2):
+        pair_landed(1, p)
     middle = (rows + TILE, rows + 2 * TILE, rows + 3 * TILE)
     normalise_rows(rows, middle[0])
-    hidden_rows(rows, middle[0], (lambda: plane_piece(2, 0), lambda: plane_piece(2, 1)))
-    split = total // 3
-
-    def end_across(p):
-        def act_on():
-            own_piece(3, p)
-            own_across(3, p)
-
-        guarded(is_end, act_on)
-
-    weight_grads(0, split, 0, 2, True)
-    end_across(0)
-    weight_grads(0, split, 2, 4, True)
-    end_across(1)
-    take_plane()
-    corner_piece(2, 0)
-    corner_piece(2, 1)
-    pair_landed(2, 0)
-    pair_landed(2, 1)
+    hidden_rows(rows, middle[0], (
+        lambda: None, lambda: None,
+        all_of(lambda: mid_corner(3, 0), lambda: plane_piece(2, 0), lambda: end_corner(2, 0)),
+    ))
+    send_plane(2)
+    weight_grads(rows, middle[0], 0, 4, False)
+    plane_piece(2, 1)
+    mid_corner(3, 1)
+    end_corner(2, 1)
+    own_across(3, 0)
+    for p in range(2):
+        pair_landed(2, p)
     normalise_rows(middle[0], middle[1])
-    hidden_rows(middle[0], middle[1])
-    finish_input()
+    hidden_rows(middle[0], middle[1], (lambda: None, lambda: end_corner(3, 0)))
+    own_across(3, 1)
     normalise_rows(middle[1], middle[2])
     hidden_rows(middle[1], middle[2])
+    end_corner(3, 1)
+    take_plane()
+    weight_grads(split, 3 * rows, 0, 2, False)
     plane_piece(3, 0)
-    weight_grads(split, 2 * split, 0, 2, False)
-    plane_piece(3, 1)
-    weight_grads(split, 2 * split, 2, 4, False)
-    corner_piece(3, 0)
+    weight_grads(split, 3 * rows, 2, 4, False)
+    finish_input()
     pair_landed(3, 0)
     normalise_rows(3 * rows, total)
-
-    def rest():
-        corner_piece(3, 1)
-        pair_landed(3, 1)
-
-    hidden_rows(3 * rows, total, (rest, lambda: None))
-    dy_tail[...] = buf[1, 2 * split:, :]
-    for make, guard in sent:
-        if guard is None:
+    hidden_rows(3 * rows, total, (lambda: plane_piece(3, 1), lambda: pair_landed(3, 1)))
+    for make, guards in sent:
+        if not guards:
             make().wait_send()
         else:
-            pl.when(guard)(lambda make=make: make().wait_send())
+            pl.when(functools.reduce(jnp.logical_and, guards))(lambda make=make: make().wait_send())
 
 
 def fused_step(tokens, cotangent, gain, w_gate, w_up, w_down):
@@ -502,21 +577,26 @@
     return pl.pallas_call(
         step_kernel,
         out_shape=[
-            pltpu.VMEM((3, hidden, width), full_type),
-            pltpu.VMEM((3, hidden, total), half_type),
-            pltpu.VMEM((total, width), half_type),
-            pltpu.VMEM((total // 3, width), half_type),
+            pltpu.VMEM((hidden, width), full_type),
+            pltpu.VMEM((hidden, width), full_type),
+            pltpu.VMEM((hidden, width), full_type),
+            pltpu.VMEM((3, hidden, rows), half_type),
+            pltpu.VMEM((rows, width), half_type),
+            pltpu.VMEM((rows, width), half_type),
             pltpu.VMEM((rows, cols), half_type),
-            pltpu.VMEM((8, cols), full_type),
+            pltpu.VMEM((1, cols), full_type),
         ],
         in_specs=[hbm] * 6,
-        out_specs=[vmem] * 6,
+        out_specs=[vmem] * 8,
         scratch_shapes=[
+            pltpu.VMEM((3, hidden, rows + TILE), half_type),
+            pltpu.VMEM((rows + TILE, width), half_type),
             pltpu.VMEM((2, total, width), half_type),
             pltpu.VMEM((3, hidden, width), half_type),
             pltpu.VMEM((1, width), full_type),
             pltpu.VMEM((rows, 128), full_type),
             pltpu.VMEM((2, rows, hidden), half_type),
+            pltpu.VMEM((4, rows, cols), full_type),
             pltpu.VMEM((4, rows, cols), half_type),
             pltpu.VMEM((4, rows, cols), half_type),
             pltpu.VMEM((rows, cols), full_type),
@@ -526,21 +606,20 @@
             pltpu.VMEM((7, 8, rows), full_type),
             pltpu.VMEM((8, cols), full_type),
             pltpu.VMEM((3, 8, cols), full_type),
-            dma((6,)), dma((12, 4, 2)), dma((4, 4, 2)), dma((2, 4, 2)), dma((4, 4, 2)),
+            dma((6,)), dma((14, 4, 2)), dma((4, 4, 2)), dma((2, 4, 2)), dma((4, 4, 2)), dma((2, 1, 2)),
             dma((4,)), dma((4,)), dma((3,)), dma((3,)), dma((7,)), dma((7,)), dma((3,)), dma((3,)),
         ],
         compiler_params=pltpu.CompilerParams(
-            collective_id=0, has_side_effects=True, vmem_limit_bytes=30 * 2**20
+            collective_id=0, has_side_effects=True, vmem_limit_bytes=37 * 2**20
         ),
         name="step",
     )(tokens, cotangent, gain.reshape(1, width), w_gate, w_up, w_down)
 
 
-def last_kernel(grads, act, nrm, dy, gi, gg, gate_ref, up_ref, down_ref, gi_ref, gg_ref, stage, sem):
+def last_kernel(grad_a, grad_b, grad_c, act, nrm, dy, gi, gg, gate_ref, up_ref, down_ref, gi_ref, gg_ref, stage, sem):
     width = nrm.shape[1]
-    count = dy.shape[0]
-    start = nrm.shape[0] - count
     step = 2 * TILE
+    grads = (grad_a, grad_b, grad_c)
     outs = (gate_ref, up_ref, down_ref)
     small = [
         pltpu.make_async_copy(gi, gi_ref, sem.at[2, 0]),
@@ -556,12 +635,12 @@
             copy.wait()
         waiting[slot] = []
         for i in range(3):
-            left = act[(i + 1) % 3, :, start:]
-            value = dy[:, span] if i == 2 else nrm[start:, span]
+            left = act[(i + 1) % 3]
+            value = dy[:, span] if i == 2 else nrm[:, span]
             product = jnp.dot(left, value, preferred_element_type=jnp.float32)
             if i == 2:
                 product = 0.5 * product
-            stage[slot, i] = grads[i, :, span] + product
+            stage[slot, i] = grads[i][:, span] + product
             copy = pltpu.make_async_copy(stage.at[slot, i], outs[i].at[:, span], sem.at[slot, i])
             copy.start()
             waiting[slot].append(copy)
@@ -580,9 +659,9 @@
         out_shape=[
             full, full, full,
             jax.ShapeDtypeStruct((rows, cols), tokens.dtype),
-            jax.ShapeDtypeStruct((8, cols), jnp.float32),
+            jax.ShapeDtypeStruct((1, cols), jnp.float32),
         ],
-        in_specs=[vmem] * 6,
+        in_specs=[vmem] * 8,
         out_specs=[pl.BlockSpec(memory_space=pltpu.HBM)] * 5,
         scratch_shapes=[
             pltpu.VMEM((2, 3, hidden, 2 * TILE), jnp.float32),

time: 101 us -> 76.5 us (0.76)
  local copies, waits for them, and re-layouts: 17.3 us -> 0 us
  Pallas kernels: 82.2 us -> 75.5 us
    unnamed x8 -> x0, local copies, waits for them, and re-layouts: 16.7 us -> none
    pallas_call x1, Pallas kernels: 75.9 us -> 69.1 us  [fused_step(): pl.pallas_call(step_kernel, out_shape=[pltpu.VMEM((hidden, width), full_t...]
where the time goes in v2:
time: 76.5 us; the launch traced here: 76.3 us
  Pallas kernels  75.5 us (99%)
  between operations  0.8 us (1%)
    pallas_call x1, Pallas kernels, fused_step(): pl.pallas_call(step_kernel, out_shape=[pltpu.VMEM((hidden, width), full_t...  69.1 us
    pallas_call x1, Pallas kernels, fused(): pl.pallas_call(last_kernel, out_shape=[full, full, full, jax.ShapeDtypeSt...  6.37 us

profile of v2, /device:TPU:0, one launch (start us, length us, event | category | flops | bytes accessed | tf_op | source)
XLA Modules:
  0.0 76.3 jit_solution(6633394251945637434)
XLA Ops:
  0.6 69.1 %step.1 = (f32[672,2048]{1,0:T(8,128)S(1)}, f32[672,2048]{1,0:T(8,128)S(1)}, f32[672,2048]{1,0:T(8,128)S(1)}, bf16[3,672,384]{2,1,0:T(8,128)(2,1)S(1)}, bf16[384...) custom-call(bf16[384,256]{1,0:T(8,128)(2,1)} %x_ref.1, ...), custom_call_target="tpu_custom_call" | custom-call | tf_op jit(solution)/shard_map/step/pallas_call | solution.py:577
  69.8 6.4 %last.1 = (f32[672,2048]{1,0:T(8,128)}, f32[672,2048]{1,0:T(8,128)}, f32[672,2048]{1,0:T(8,128)}, bf16[384,256]{1,0:T(8,128)(2,1)}, f32[1,256]{1,0:T(1,128)}) custom-call(f32[672,2048]{1,0:T(8,128)S(1)} %get-tuple-element.18.grad_a, f32[672,2048]{1,0:T(8,128)S(1)} %get-tuple-element.19.grad_b, f32[672,2048]{1,0:T(8,128)S(1)} %get-tuple-element.20.grad_c, ...), custom_call_target="tpu_custom_call" | custom-call | tf_op jit(solution)/shard_map/last/pallas_call | solution.py:657

commit v3 on v2

--- a/solution.py
+++ b/solution.py
@@ -99,7 +99,7 @@
     grad_a, grad_b, grad_c, act_tail, nrm_tail, dy_tail, gi_ref, gg_ref,
     act_main, nrm_main, buf, wts, gain, inv, turned, own_part, pair_out, pair_in, own_sum, plane_out, plane_in,
     row_out, row_in, gain_out, gain_in,
-    load_sem, send_sem, recv_sem, corner_sem, pair_sem, late_sem,
+    load_sem, send_sem, recv_sem, line_own, line_corner, corner_sem, pair_sem, late_sem,
     give_sem, take_sem, block_send, block_recv, row_send, row_recv, gain_send, gain_recv,
 ):
     z, y, t = lax.axis_index("rep"), lax.axis_index("fs"), lax.axis_index("tp")
@@ -140,6 +140,11 @@
 
     grads = (grad_a, grad_b, grad_c)
     sent = []
+    numbers = {}
+
+    def number(*key):
+        return numbers.setdefault(key, len(numbers))
+
 
     def send(make, guard=None):
         if guard is None:
@@ -156,14 +161,16 @@
 
     def arrive(ref, sem):
         pltpu.make_async_remote_copy(
-            src_ref=ref, dst_ref=ref, send_sem=send_sem.at[0, 0, 0], recv_sem=sem,
+            src_ref=ref, dst_ref=ref, send_sem=send_sem.at[0], recv_sem=sem,
             device_id=pair_id, device_id_type=MESH,
         ).wait_recv()
 
     def move(slot, q, p, kind, lands, target, start=0, size=rows):
+        own_number = number(kind, slot, p)
+
         def make():
             ref = piece(slot, column[q], p, start, size)
-            return remote(ref, ref, send_sem.at[kind, slot, p], lands[0].at[lands[1], slot, p], target)
+            return remote(ref, ref, send_sem.at[own_number], lands[0].at[lands[1], slot, p], target)
 
         send(make)
 
@@ -171,16 +178,16 @@
         move(slot, q, p, q, (pair_sem, q), pair_id)
 
     def to_x(slot, p):
-        move(slot, OWN, p, 4, (recv_sem, ACROSS_X), x_id)
+        move(slot, OWN, p, 4, (recv_sem, 0), x_id)
 
     def to_y(slot, p):
-        move(slot, OWN, p, 5, (recv_sem, ACROSS_Y), y_id)
+        move(slot, OWN, p, 5, (recv_sem, 1), y_id)
 
     def split_across(p, first):
         a, b = (0, half) if first else (half, 0)
         if first:
-            move(0, OWN, p, 4, (recv_sem, ACROSS_X), x_id, a, half)
-            move(0, OWN, p, 5, (recv_sem, ACROSS_Y), y_id, b, half)
+            move(0, OWN, p, 4, (recv_sem, 0), x_id, a, half)
+            move(0, OWN, p, 5, (recv_sem, 1), y_id, b, half)
         else:
             move(0, OWN, p, 12, (late_sem, 0), x_id, a, half)
             move(0, OWN, p, 13, (late_sem, 1), y_id, b, half)
@@ -190,10 +197,13 @@
         move(slot, ACROSS_Y, p, 7, (corner_sem, 1), x_id, half, half)
 
     def along(slot, q, p, there, kind, target, guard):
+        own_number = number(kind, slot, p)
+        line = line_own if q == OWN else line_corner
+
         def make():
             return remote(
                 piece(slot, column[q], p), piece(there, column[q], p),
-                send_sem.at[kind, slot, p], recv_sem.at[q, there, p], target,
+                send_sem.at[own_number], line.at[there - 1, p], target,
             )
 
         send(make, guard)
@@ -205,7 +215,11 @@
         along(slot, q, p, there, 10 if q == OWN else 11, outer_id, is_mid)
 
     def landed(slot, q, p):
-        arrive(piece(slot, column[q], p), recv_sem.at[q, slot, p])
+        if q in (ACROSS_X, ACROSS_Y):
+            sem = recv_sem.at[q - 1, slot, p]
+        else:
+            sem = (line_own if q == OWN else line_corner).at[slot - 1, p]
+        arrive(piece(slot, column[q], p), sem)
 
     def corner_landed(slot, p):
         arrive(piece(slot, column[CORNER], p, 0, half), corner_sem.at[0, slot, p])
@@ -233,8 +247,8 @@
         to_y(slot, p)
 
     def split_landed(p):
-        arrive(piece(0, column[ACROSS_X], p, 0, half), recv_sem.at[ACROSS_X, 0, p])
-        arrive(piece(0, column[ACROSS_Y], p, half, half), recv_sem.at[ACROSS_Y, 0, p])
+        arrive(piece(0, column[ACROSS_X], p, 0, half), recv_sem.at[0, 0, p])
+        arrive(piece(0, column[ACROSS_Y], p, half, half), recv_sem.at[1, 0, p])
         relay(0, p)
 
     def split_rest(p):
@@ -517,9 +531,9 @@
     ))
     give_pair()
     mid_corner(2, 1)
-    weight_grads(0, rows, 0, 1, True)
     plane_piece(1, 1)
     end_across()
+    weight_grads(0, rows, 0, 1, True)
     last_own(0)
     give_plane()
     end_corner(1, 0)
@@ -529,36 +543,36 @@
     weight_grads(0, rows, 3, 4, True)
     send_plane(0)
     send_plane(1)
-    for p in range(2):
-        pair_landed(1, p)
+    pair_landed(1, 0)
     middle = (rows + TILE, rows + 2 * TILE, rows + 3 * TILE)
     normalise_rows(rows, middle[0])
     hidden_rows(rows, middle[0], (
-        lambda: None, lambda: None,
+        lambda: None, lambda: pair_landed(1, 1),
         all_of(lambda: mid_corner(3, 0), lambda: plane_piece(2, 0), lambda: end_corner(2, 0)),
     ))
     send_plane(2)
-    weight_grads(rows, middle[0], 0, 4, False)
+    weight_grads(rows, middle[0], 0, 2, False)
+    own_across(3, 0)
+    weight_grads(rows, middle[0], 2, 4, False)
+    pair_landed(2, 0)
+    normalise_rows(middle[0], middle[1])
     plane_piece(2, 1)
     mid_corner(3, 1)
     end_corner(2, 1)
-    own_across(3, 0)
-    for p in range(2):
-        pair_landed(2, p)
-    normalise_rows(middle[0], middle[1])
-    hidden_rows(middle[0], middle[1], (lambda: None, lambda: end_corner(3, 0)))
+    hidden_rows(middle[0], middle[1], (lambda: None, all_of(lambda: end_corner(3, 0), lambda: pair_landed(2, 1))))
     own_across(3, 1)
     normalise_rows(middle[1], middle[2])
     hidden_rows(middle[1], middle[2])
     end_corner(3, 1)
     take_plane()
-    weight_grads(split, 3 * rows, 0, 2, False)
+    weight_grads(split, 3 * rows, 0, 3, False)
     plane_piece(3, 0)
-    weight_grads(split, 3 * rows, 2, 4, False)
-    finish_input()
+    weight_grads(split, 3 * rows, 3, 4, False)
     pair_landed(3, 0)
     normalise_rows(3 * rows, total)
-    hidden_rows(3 * rows, total, (lambda: plane_piece(3, 1), lambda: pair_landed(3, 1)))
+    hidden_rows(3 * rows, total, (
+        lambda: plane_piece(3, 1), all_of(finish_input, lambda: pair_landed(3, 1)),
+    ))
     for make, guards in sent:
         if not guards:
             make().wait_send()
@@ -606,7 +620,8 @@
             pltpu.VMEM((7, 8, rows), full_type),
             pltpu.VMEM((8, cols), full_type),
             pltpu.VMEM((3, 8, cols), full_type),
-            dma((6,)), dma((14, 4, 2)), dma((4, 4, 2)), dma((2, 4, 2)), dma((4, 4, 2)), dma((2, 1, 2)),
+            dma((6,)), dma((76,)), dma((2, 4, 2)), dma((3, 2)), dma((3, 2)),
+            dma((2, 2, 2)), dma((4, 4, 2)), dma((2, 1, 2)),
             dma((4,)), dma((4,)), dma((3,)), dma((3,)), dma((7,)), dma((7,)), dma((3,)), dma((3,)),
         ],
         compiler_params=pltpu.CompilerParams(

time: 76.5 us -> 72.2 us (0.944)
  Pallas kernels: 75.5 us -> 71.2 us
    pallas_call x1, Pallas kernels: 69.1 us -> 64.8 us  [fused_step(): pl.pallas_call(step_kernel, out_shape=[pltpu.VMEM((hidden, width), full_t...]
where the time goes in v3:
time: 72.2 us; the launch traced here: 72 us
  Pallas kernels  71.2 us (99%)
  between operations  0.82 us (1%)
    pallas_call x1, Pallas kernels, fused_step(): pl.pallas_call(step_kernel, out_shape=[pltpu.VMEM((hidden, width), full_t...  64.8 us
    pallas_call x1, Pallas kernels, fused(): pl.pallas_call(last_kernel, out_shape=[full, full, full, jax.ShapeDtypeSt...  6.38 us

profile of v3, /device:TPU:0, one launch (start us, length us, event | category | flops | bytes accessed | tf_op | source)
XLA Modules:
  0.0 72.0 jit_solution(6925046214313555270)
XLA Ops:
  0.6 64.8 %step.1 = (f32[672,2048]{1,0:T(8,128)S(1)}, f32[672,2048]{1,0:T(8,128)S(1)}, f32[672,2048]{1,0:T(8,128)S(1)}, bf16[3,672,384]{2,1,0:T(8,128)(2,1)S(1)}, bf16[384...) custom-call(bf16[384,256]{1,0:T(8,128)(2,1)} %x_ref.1, ...), custom_call_target="tpu_custom_call" | custom-call | tf_op jit(solution)/shard_map/step/pallas_call | solution.py:591
  65.5 6.4 %last.1 = (f32[672,2048]{1,0:T(8,128)}, f32[672,2048]{1,0:T(8,128)}, f32[672,2048]{1,0:T(8,128)}, bf16[384,256]{1,0:T(8,128)(2,1)}, f32[1,256]{1,0:T(1,128)}) custom-call(f32[672,2048]{1,0:T(8,128)S(1)} %get-tuple-element.18.grad_a, f32[672,2048]{1,0:T(8,128)S(1)} %get-tuple-element.19.grad_b, f32[672,2048]{1,0:T(8,128)S(1)} %get-tuple-element.20.grad_c, ...), custom_call_target="tpu_custom_call" | custom-call | tf_op jit(solution)/shard_map/last/pallas_call | solution.py:672

commit v4 on v3

--- a/solution.py
+++ b/solution.py
@@ -262,8 +262,8 @@
         landed(slot, ACROSS_Y, p)
         if slot == 0:
             relay(0, p)
-        elif slot == 1:
-            guarded(is_end, lambda: relay(1, p))
+        elif slot == 1 and p == 0:
+            guarded(is_end, lambda: relay(1, 0))
         to_pair(slot, ACROSS_X, p)
         to_pair(slot, ACROSS_Y, p)
 
@@ -271,7 +271,9 @@
         if slot == 0:
             corner_landed(0, p)
             to_inner(0, CORNER, p, inner_slot)
-        elif slot == 1:
+            if p == 1:
+                to_outer(0, CORNER, 1, 1)
+        elif slot == 1 and p == 0:
             pl.when(is_end)(lambda: corner_landed(1, p))
 
             def passed_on():
@@ -508,9 +510,6 @@
         for p in range(2):
             guarded(is_end, lambda: own_across(2, p))
 
-    def last_own(p):
-        either(lambda: own_piece(3, p), lambda: corner_piece(1, p))
-
     def mid_corner(slot, p):
         guarded(is_mid, lambda: corner_piece(slot, p))
 
@@ -534,40 +533,43 @@
     plane_piece(1, 1)
     end_across()
     weight_grads(0, rows, 0, 1, True)
-    last_own(0)
+    mid_corner(1, 0)
     give_plane()
     end_corner(1, 0)
+    end_corner(1, 1)
     weight_grads(0, rows, 1, 3, True)
-    last_own(1)
-    end_corner(1, 1)
+    guarded(is_end, lambda: own_piece(3, 0))
+    mid_corner(1, 1)
     weight_grads(0, rows, 3, 4, True)
     send_plane(0)
     send_plane(1)
     pair_landed(1, 0)
     middle = (rows + TILE, rows + 2 * TILE, rows + 3 * TILE)
     normalise_rows(rows, middle[0])
-    hidden_rows(rows, middle[0], (
-        lambda: None, lambda: pair_landed(1, 1),
-        all_of(lambda: mid_corner(3, 0), lambda: plane_piece(2, 0), lambda: end_corner(2, 0)),
-    ))
+    hidden_rows(rows, middle[0], (lambda: None, lambda: pair_landed(1, 1)))
+    guarded(is_end, lambda: own_piece(3, 1))
+    mid_corner(3, 0)
+    plane_piece(2, 0)
     send_plane(2)
     weight_grads(rows, middle[0], 0, 2, False)
     own_across(3, 0)
     weight_grads(rows, middle[0], 2, 4, False)
+    end_corner(2, 0)
     pair_landed(2, 0)
-    normalise_rows(middle[0], middle[1])
+    normalise_rows(middle[0], middle[2])
     plane_piece(2, 1)
     mid_corner(3, 1)
     end_corner(2, 1)
-    hidden_rows(middle[0], middle[1], (lambda: None, all_of(lambda: end_corner(3, 0), lambda: pair_landed(2, 1))))
-    own_across(3, 1)
-    normalise_rows(middle[1], middle[2])
-    hidden_rows(middle[1], middle[2])
-    end_corner(3, 1)
+    hidden_rows(middle[0], middle[2], (
+        lambda: None,
+        all_of(lambda: own_across(3, 1), lambda: pair_landed(2, 1)),
+    ))
+    end_corner(3, 0)
     take_plane()
     weight_grads(split, 3 * rows, 0, 3, False)
     plane_piece(3, 0)
     weight_grads(split, 3 * rows, 3, 4, False)
+    end_corner(3, 1)
     pair_landed(3, 0)
     normalise_rows(3 * rows, total)
     hidden_rows(3 * rows, total, (

time: 72.2 us -> 71.3 us (0.988)
  Pallas kernels: 71.2 us -> 70.3 us
    pallas_call x1, Pallas kernels: 64.8 us -> 63.9 us  [fused_step(): pl.pallas_call(step_kernel, out_shape=[pltpu.VMEM((hidden, width), full_t...]
where the time goes in v4:
time: 71.3 us; the launch traced here: 71.1 us
  Pallas kernels  70.3 us (99%)
  between operations  0.82 us (1%)
    pallas_call x1, Pallas kernels, fused_step(): pl.pallas_call(step_kernel, out_shape=[pltpu.VMEM((hidden, width), full_t...  63.9 us
    pallas_call x1, Pallas kernels, fused(): pl.pallas_call(last_kernel, out_shape=[full, full, full, jax.ShapeDtypeSt...  6.37 us

profile of v4, /device:TPU:0, one launch (start us, length us, event | category | flops | bytes accessed | tf_op | source)
XLA Modules:
  0.0 71.1 jit_solution(10101693639208441403)
XLA Ops:
  0.6 63.9 %step.1 = (f32[672,2048]{1,0:T(8,128)S(1)}, f32[672,2048]{1,0:T(8,128)S(1)}, f32[672,2048]{1,0:T(8,128)S(1)}, bf16[3,672,384]{2,1,0:T(8,128)(2,1)S(1)}, bf16[384...) custom-call(bf16[384,256]{1,0:T(8,128)(2,1)} %x_ref.1, ...), custom_call_target="tpu_custom_call" | custom-call | tf_op jit(solution)/shard_map/step/pallas_call | solution.py:593
  64.6 6.4 %last.1 = (f32[672,2048]{1,0:T(8,128)}, f32[672,2048]{1,0:T(8,128)}, f32[672,2048]{1,0:T(8,128)}, bf16[384,256]{1,0:T(8,128)(2,1)}, f32[1,256]{1,0:T(1,128)}) custom-call(f32[672,2048]{1,0:T(8,128)S(1)} %get-tuple-element.18.grad_a, f32[672,2048]{1,0:T(8,128)S(1)} %get-tuple-element.19.grad_b, f32[672,2048]{1,0:T(8,128)S(1)} %get-tuple-element.20.grad_c, ...), custom_call_target="tpu_custom_call" | custom-call | tf_op jit(solution)/shard_map/last/pallas_call | solution.py:674
